TPU v7x, 32 devices: a whole 2x2x4 slice. The times are simulated.
32 devices in a mesh: ra: 4 (over z), cb: 8 (over y, x, core).
Axes of the slice: x: 2, y: 2, z: 4, core: 2. Of those that a mesh axis runs over, the one named last changes fastest.
Arguments:
- tokens: bfloat16 [2, 128, 3072], P(None, None, 'ra'), may hold values from -70 to 70
- norm_gain: float32 [2, 3072], P(None, 'ra'), may hold values from 0.1 to 1.9
- gate_weight: float32 [2, 3072, 8448], P(None, 'ra', 'cb'), may hold values from -0.109375 to 0.109375
- gate_scale: float32 [2, 8448], P(None, 'cb'), may hold values from 0.5 to 2
- up_weight: float32 [2, 3072, 8448], P(None, 'ra', 'cb'), may hold values from -0.109375 to 0.109375
- up_scale: float32 [2, 8448], P(None, 'cb'), may hold values from 0.5 to 2
- conv_weight: float32 [2, 3, 8448], P(None, None, 'cb'), may hold values from -3.5 to 3.5
- conv_bias: float32 [2, 8448], P(None, 'cb'), may hold values from -3 to 3
- down_weight: float32 [2, 8448, 3072], P(None, 'cb', 'ra'), may hold values from -0.0625 to 0.0625
- down_scale: float32 [2, 3072], P(None, 'ra'), may hold values from 0.5 to 2
Outputs:
- layer_output: bfloat16 [2, 128, 3072], P(None, None, 'ra')
All inputs are finite; a program needn't handle non-finite values.
Results may differ from a plain program's by a relative error of at most 0.014.
Values may be sent and summed in bfloat16 or wider, within the bound.
A program may use at most 64 MiB of HBM per device.

v0:
```python
import functools

import jax
import jax.numpy as jnp
from jax import lax
from jax.experimental import pallas as pl
from jax.experimental.pallas import tpu as pltpu
from jax.sharding import PartitionSpec as P

eps = 1e-06
residual_keep = 0.5


def causal_mix(gate_seq, conv_taps, conv_shift):
    count = conv_taps.shape[0]
    length = gate_seq.shape[1]
    padded = jnp.pad(gate_seq, ((0, 0), (count - 1, 0), (0, 0)))
    running = jnp.zeros_like(gate_seq) + conv_shift[None, None, :]
    for offset in range(count):
        running = (
            running + conv_taps[offset][None, None, :] * padded[:, offset : offset + length, :]
        )
    return running


def sublayer(current, norm_g, gate_w, gate_s, up_w, up_s, conv_taps, conv_shift, down_w, down_s):
    sequences, length, local_width = current.shape
    row_count = sequences * length
    values = current.astype(jnp.float32).reshape(row_count, local_width)
    squares = jnp.sum(values * values, axis=1)
    scaled = (values * norm_g[None, :]).astype(jnp.bfloat16)
    gate_part = jnp.dot(scaled, gate_w.astype(jnp.bfloat16), preferred_element_type=jnp.float32)
    up_part = jnp.dot(scaled, up_w.astype(jnp.bfloat16), preferred_element_type=jnp.float32)
    gate_sum, up_sum = (
        lax.psum_scatter(gate_part, "ra", scatter_dimension=1, tiled=True),
        lax.psum_scatter(up_part, "ra", scatter_dimension=1, tiled=True),
    )
    square_sum = lax.psum(squares, "ra")
    share_cols = gate_sum.shape[1]
    col_start = lax.axis_index("ra") * share_cols
    col_gate = lax.dynamic_slice_in_dim(gate_s, col_start, share_cols, 0)
    col_up = lax.dynamic_slice_in_dim(up_s, col_start, share_cols, 0)
    used_taps = lax.dynamic_slice_in_dim(conv_taps, col_start, share_cols, 1)
    used_shift = lax.dynamic_slice_in_dim(conv_shift, col_start, share_cols, 0)
    inverse_rms = lax.rsqrt(square_sum / (local_width * lax.axis_size("ra")) + eps)[:, None]
    gate_sum = gate_sum * inverse_rms * col_gate[None, :]
    up_sum = up_sum * inverse_rms * col_up[None, :]
    units = gate_sum.shape[1]
    conv_out = causal_mix(gate_sum.reshape(sequences, length, units), used_taps, used_shift)
    hidden_act = (jax.nn.silu(conv_out) * up_sum.reshape(sequences, length, units)).astype(
        jnp.bfloat16
    )
    hidden_act = hidden_act.reshape(row_count, units)
    hidden_act = lax.all_gather(hidden_act, "ra", axis=1, tiled=True)
    down_part = jnp.dot(hidden_act, down_w.astype(jnp.bfloat16), preferred_element_type=jnp.float32)
    down_sum = lax.psum(down_part, "cb")
    branch = down_sum * down_s[None, :]
    return (
        (residual_keep * values + branch)
        .astype(jnp.bfloat16)
        .reshape(sequences, length, local_width)
    )


def shards(
    tokens,
    norm_gain,
    gate_weight,
    gate_scale,
    up_weight,
    up_scale,
    conv_weight,
    conv_bias,
    down_weight,
    down_scale,
):
    current = tokens
    for layer_index in range(2):
        current = sublayer(
            current,
            norm_gain[layer_index],
            gate_weight[layer_index],
            gate_scale[layer_index],
            up_weight[layer_index],
            up_scale[layer_index],
            conv_weight[layer_index],
            conv_bias[layer_index],
            down_weight[layer_index],
            down_scale[layer_index],
        )
    return current


MESH = pl.DeviceIdType.MESH
LANES = 128
CHUNKS = 8
LAG = dict(enter=0, mix=2, act=3, down=4, fold=6, done=8)
ORDER = ("done", "mix", "enter", "act", "fold", "down")
GAP = 8


def fused(
    chunks,
    ra,
    cb,
    tokens,
    norm_gain,
    gate_weight,
    gate_scale,
    up_weight,
    up_scale,
    conv_weight,
    conv_bias,
    down_weight,
    down_scale,
    out,
    stage_gate,
    stage_up,
    stage_down,
    in_w,
    out_w,
    state,
    own_part,
    near_part,
    far_send,
    far_part,
    hidden,
    down_part,
    down_recv,
    conv_pad,
    params,
    load_sem,
    near_s,
    near_r,
    far_s,
    far_r,
    hid_s,
    hid_r,
    red_s,
    red_r,
    out_s,
    out_r,
):
    layers = 2
    sequences, length, width = tokens.shape
    units = gate_weight.shape[1]
    main = units // LANES * LANES
    rem = units - main
    total_cols = 2 * main + LANES
    step = length // chunks
    rows = sequences * step
    items = layers * chunks
    share_rows, share_cols = down_recv.shape[2], down_recv.shape[3]
    col_parts = width // share_cols
    me = lax.axis_index("ra")
    mine = lax.axis_index("cb")
    inner = jnp.logical_and(me >= 1, me <= 2)
    outer = jnp.logical_not(inner)
    own_seq = me - 1

    loads = []
    for layer in range(layers):
        for kind, (src, dst) in enumerate(
            ((gate_weight, stage_gate), (up_weight, stage_up), (down_weight, stage_down))
        ):
            loads.append(
                pltpu.make_async_copy(src.at[layer], dst.at[layer], load_sem.at[layer * 3 + kind])
            )
    for load in loads:
        load.start()

    barrier = pltpu.get_barrier_semaphore()
    for d in range(1, ra):
        pl.semaphore_signal(
            barrier, inc=1, device_id={"ra": lax.rem(me + d, ra)}, device_id_type=MESH
        )
    for d in range(1, cb):
        pl.semaphore_signal(
            barrier, inc=1, device_id={"cb": lax.rem(mine + d, cb)}, device_id_type=MESH
        )

    for c in range(chunks):
        for s in range(sequences):
            state[c, s * step : (s + 1) * step, :] = tokens[
                s, c * step : (c + 1) * step, :
            ].astype(state.dtype)

    def convert_in(layer):
        loads[layer * 3].wait()
        loads[layer * 3 + 1].wait()
        block = 32

        @pl.loop(0, main // block)
        def _(i):
            r = pl.ds(pl.multiple_of(i * block, block), block)
            r2 = pl.ds(pl.multiple_of(main + i * block, block), block)
            in_w[layer, r, :] = stage_gate[layer, r, :].astype(jnp.bfloat16)
            in_w[layer, r2, :] = stage_up[layer, r, :].astype(jnp.bfloat16)

        first = 2 * main
        if rem:
            in_w[layer, first : first + rem, :] = stage_gate[layer, main:, :].astype(jnp.bfloat16)
            in_w[layer, first + rem : first + 2 * rem, :] = stage_up[layer, main:, :].astype(
                jnp.bfloat16
            )
        in_w[layer, first + 2 * rem :, :] = jnp.zeros((LANES - 2 * rem, width), jnp.bfloat16)

    def convert_out(layer):
        loads[layer * 3 + 2].wait()
        block = 32

        @pl.loop(0, units // block)
        def _(i):
            r = pl.ds(pl.multiple_of(i * block, block), block)
            out_w[layer, r, :] = stage_down[layer, r, :].astype(jnp.bfloat16)

        pad = out_w.shape[1] - units
        if pad:
            out_w[layer, units:, :] = jnp.zeros((pad, width), jnp.bfloat16)

    for layer in range(layers):
        lines = [gate_scale[layer : layer + 1, :], up_scale[layer : layer + 1, :]]
        lines.append(conv_bias[layer : layer + 1, :])
        lines += [conv_weight[j, layer : layer + 1, :] for j in range(conv_weight.shape[0])]
        for row, line in enumerate(lines):
            if rem:
                zeros = jnp.zeros((1, LANES - rem), jnp.float32)
                params[layer, row : row + 1, main:] = jnp.concatenate(
                    [line[:, main:], zeros], axis=1
                )
            params[layer, row : row + 1, :main] = line[:, :main]

    lane = lax.broadcasted_iota(jnp.int32, (1, LANES), 1)

    def put_squares(tile, squares):
        high = squares.astype(jnp.bfloat16).astype(jnp.float32)
        low = squares - high
        return jnp.where(lane == 2 * rem, high, jnp.where(lane == 2 * rem + 1, low, tile))

    def get_squares(tile):
        keep = jnp.logical_and(lane >= 2 * rem, lane < 2 * rem + 2)
        return jnp.sum(jnp.where(keep, tile, 0.0), axis=1, keepdims=True)

    def near_copy(k, first):
        to = jnp.where(me == 0, 1, 2)
        passed = jnp.where(me < 2, 1, 0)
        r = hid_rows(passed if first else 1 - passed)
        return pltpu.make_async_remote_copy(
            src_ref=own_part.at[k, r],
            dst_ref=near_part.at[k, r],
            send_sem=near_s.at[k, int(first)],
            recv_sem=near_r.at[k, int(first)],
            device_id={"ra": to},
            device_id_type=MESH,
        )

    def far_copy(k):
        return pltpu.make_async_remote_copy(
            src_ref=far_send.at[k],
            dst_ref=far_part.at[k],
            send_sem=far_s.at[k],
            recv_sem=far_r.at[k],
            device_id={"ra": 3 - me},
            device_id_type=MESH,
        )

    def hid_rows(seq):
        return pl.ds(pl.multiple_of(seq * step, step), step)

    def hid_copy(k, d, seq):
        return pltpu.make_async_remote_copy(
            src_ref=hidden.at[k, hid_rows(seq)],
            dst_ref=hidden.at[k, hid_rows(seq)],
            send_sem=hid_s.at[k, d - 1],
            recv_sem=hid_r.at[k, seq],
            device_id={"ra": lax.rem(me + d, ra)},
            device_id_type=MESH,
        )

    def share(p):
        return (
            pl.ds(pl.multiple_of(p // col_parts * share_rows, share_rows), share_rows),
            pl.ds(pl.multiple_of(p % col_parts * share_cols, LANES), share_cols),
        )

    def red_copy(k, d):
        to = lax.rem(mine + d, cb)
        r, c = share(to)
        return pltpu.make_async_remote_copy(
            src_ref=down_part.at[k, r, c],
            dst_ref=down_recv.at[k, d - 1],
            send_sem=red_s.at[k, d - 1],
            recv_sem=red_r.at[k, d - 1],
            device_id={"cb": to},
            device_id_type=MESH,
        )

    def out_copy(k, d, owner):
        r, c = share(owner)
        return pltpu.make_async_remote_copy(
            src_ref=state.at[k + chunks, r, c],
            dst_ref=state.at[k + chunks, r, c],
            send_sem=out_s.at[k, d - 1],
            recv_sem=out_r.at[k, d - 1],
            device_id={"cb": lax.rem(mine + d, cb)},
            device_id_type=MESH,
        )

    def enter(k):
        layer = k // chunks
        values = state[k].astype(jnp.float32)
        squares = jnp.sum(values * values, axis=1, keepdims=True)
        gain = norm_gain[pl.ds(layer, 1), :]
        scaled = (values * gain).astype(jnp.bfloat16)
        block = 512
        for start in range(0, 2 * main, block):
            stop = min(start + block, 2 * main)
            own_part[k, :, start:stop] = lax.dot_general(
                scaled,
                in_w[layer, start:stop, :],
                (((1,), (1,)), ((), ())),
                preferred_element_type=jnp.float32,
            ).astype(jnp.bfloat16)
        tile = lax.dot_general(
            scaled,
            in_w[layer, 2 * main :, :],
            (((1,), (1,)), ((), ())),
            preferred_element_type=jnp.float32,
        )
        own_part[k, :, 2 * main :] = put_squares(tile, squares).astype(jnp.bfloat16)

        @pl.when(outer)
        def _():
            near_copy(k, True).start()
            near_copy(k, False).start()

    def mix(k):
        near_copy(k, True).wait_recv()
        r = hid_rows(1 - own_seq)
        both = own_part[k, r, : 2 * main].astype(jnp.float32) + near_part[
            k, r, : 2 * main
        ].astype(jnp.float32)
        far_send[k, :, : 2 * main] = both.astype(jnp.bfloat16)
        tile = own_part[k, r, 2 * main :].astype(jnp.float32) + near_part[k, r, 2 * main :].astype(
            jnp.float32
        )
        far_send[k, :, 2 * main :] = put_squares(tile, get_squares(tile)).astype(jnp.bfloat16)
        far_copy(k).start()

    def act(k):
        layer = k // chunks
        near_copy(k, False).wait_recv()
        far_copy(k).wait_recv()
        r = hid_rows(own_seq)

        def total(start, stop):
            return (
                own_part[k, r, start:stop].astype(jnp.float32)
                + near_part[k, r, start:stop].astype(jnp.float32)
                + far_part[k, :, start:stop].astype(jnp.float32)
            )

        tile = total(2 * main, total_cols)
        inverse_rms = lax.rsqrt(get_squares(tile) / (width * ra) + eps)

        @pl.when(k % chunks == 0)
        def _():
            conv_pad[0:8, :] = jnp.zeros((8, conv_pad.shape[1]), jnp.float32)

        def piece(gate, up, start, stop):
            def param(row):
                return params[layer, row : row + 1, start:stop]

            conv_pad[8 : 8 + step, start:stop] = gate * inverse_rms * param(0)
            conv = param(2)
            taps = conv_weight.shape[0]
            for j in range(taps):
                first = 8 - (taps - 1) + j
                conv = conv + param(3 + j) * conv_pad[first : first + step, start:stop]
            conv_pad[0:8, start:stop] = conv_pad[step : step + 8, start:stop]
            value = conv / (1.0 + jnp.exp(-conv)) * (up * inverse_rms * param(1))
            hidden[k, r, start:stop] = value.astype(jnp.bfloat16)

        block = 256
        for start in range(0, main, block):
            stop = min(start + block, main)
            piece(total(start, stop), total(main + start, main + stop), start, stop)
        if rem:
            piece(tile, pltpu.roll(tile, LANES - rem, axis=1), main, main + LANES)
        for d in (2, 1, 3):
            hid_copy(k, d, own_seq).start()

    def down(k):
        layer = k // chunks
        for seq in range(sequences):

            @pl.when(jnp.logical_not(jnp.logical_and(inner, own_seq == seq)))
            def _():
                hid_copy(k, 1, seq).wait_recv()

        down_part[k] = jnp.dot(
            hidden[k], out_w[layer], preferred_element_type=jnp.float32
        ).astype(down_part.dtype)
        for d in range(1, cb):
            red_copy(k, d).start()

    def fold(k):
        layer = k // chunks
        r, c = share(mine)
        total = down_part[k, r, c].astype(jnp.float32)
        for d in range(1, cb):
            red_copy(k, d).wait_recv()
            total = total + down_recv[k, d - 1].astype(jnp.float32)
        kept = residual_keep * state[k, r, c].astype(jnp.float32)
        state[k + chunks, r, c] = (
            (kept + total * down_scale[pl.ds(layer, 1), c])
            .astype(jnp.bfloat16)
            .astype(state.dtype)
        )
        for d in range(1, cb):
            out_copy(k, d, mine).start()

    def done(k):
        for d in range(1, cb):
            out_copy(k, d, lax.rem(mine - d + cb, cb)).wait_recv()

    convert_in(0)
    pl.semaphore_wait(barrier, ra - 1 + cb - 1)

    works = dict(enter=enter, mix=mix, act=act, down=down, fold=fold, done=done)

    @pl.loop(0, GAP + chunks + max(LAG.values()))
    def _(slot):
        for name in ORDER:
            place = slot - LAG[name]
            late = place >= GAP
            item = jnp.where(late, place - GAP + chunks, place)
            good = jnp.logical_and(item >= 0, item < jnp.where(late, items, chunks))
            if name in ("mix", "act"):
                good = jnp.logical_and(good, inner)

            @pl.when(good)
            def _():
                works[name](item)

            if name == "enter":

                @pl.when(slot == 0)
                def _():
                    convert_out(0)

                @pl.when(slot == 1)
                def _():
                    convert_in(1)

                @pl.when(slot == 2)
                def _():
                    convert_out(1)

    for c in range(chunks):
        for s in range(sequences):
            out[s, c * step : (c + 1) * step, :] = state[
                items + c, s * step : (s + 1) * step, :
            ].astype(jnp.bfloat16)

    @pl.loop(0, items)
    def _(k):
        @pl.when(outer)
        def _():
            near_copy(k, True).wait_send()
            near_copy(k, False).wait_send()

        @pl.when(inner)
        def _():
            far_copy(k).wait_send()
            for d in range(1, ra):
                hid_copy(k, d, own_seq).wait_send()

        for d in range(1, cb):
            red_copy(k, d).wait_send()
            out_copy(k, d, mine).wait_send()


def share_shape(rows, width, parts):
    for tile, dtype in ((16, jnp.bfloat16), (8, jnp.float32)):
        for col_parts in range(1, parts + 1):
            if parts % col_parts or width % (col_parts * LANES):
                continue
            if rows % (parts // col_parts * tile) == 0:
                return (rows * col_parts // parts, width // col_parts), dtype
    return None


def fused_shards(ra, cb, chunks, *operands):
    tokens, gate_weight = operands[0], operands[2]
    layers = 2
    sequences, length, width = tokens.shape
    units = gate_weight.shape[2]
    main = units // LANES * LANES
    total_cols = 2 * main + LANES
    padded = main + (LANES if units > main else 0)
    step = length // chunks
    rows = sequences * step
    items = layers * chunks
    part, part_type = share_shape(rows, width, cb)
    vmem = pl.BlockSpec(memory_space=pltpu.VMEM)
    hbm = pl.BlockSpec(memory_space=pl.ANY)
    dma = pltpu.SemaphoreType.DMA
    bf16, f32 = jnp.bfloat16, jnp.float32
    return pl.pallas_call(
        functools.partial(fused, chunks, ra, cb),
        out_shape=jax.ShapeDtypeStruct(tokens.shape, tokens.dtype),
        in_specs=[vmem, vmem, hbm, vmem, hbm, vmem, vmem, vmem, hbm, vmem],
        out_specs=vmem,
        scratch_shapes=[
            pltpu.VMEM((layers, units, width), f32),
            pltpu.VMEM((layers, units, width), f32),
            pltpu.VMEM((layers, units, width), f32),
            pltpu.VMEM((layers, total_cols, width), bf16),
            pltpu.VMEM((layers, padded, width), bf16),
            pltpu.VMEM((items + chunks, rows, width), part_type),
            pltpu.VMEM((items, rows, total_cols), bf16),
            pltpu.VMEM((items, rows, total_cols), bf16),
            pltpu.VMEM((items, step, total_cols), bf16),
            pltpu.VMEM((items, step, total_cols), bf16),
            pltpu.VMEM((items, rows, padded), bf16),
            pltpu.VMEM((items, rows, width), part_type),
            pltpu.VMEM((items, cb - 1) + part, part_type),
            pltpu.VMEM((8 + step, padded), f32),
            pltpu.VMEM((layers, 3 + operands[6].shape[1], padded), f32),
            dma((layers * 3,)),
            dma((items, sequences)),
            dma((items, sequences)),
            dma((items,)),
            dma((items,)),
            dma((items, ra - 1)),
            dma((items, sequences)),
            dma((items, cb - 1)),
            dma((items, cb - 1)),
            dma((items, cb - 1)),
            dma((items, cb - 1)),
        ],
        compiler_params=pltpu.CompilerParams(
            collective_id=0, has_side_effects=True, vmem_limit_bytes=60 * 1024 * 1024
        ),
    )(
        *operands[:2],
        jnp.swapaxes(gate_weight, 1, 2),
        operands[3],
        jnp.swapaxes(operands[4], 1, 2),
        operands[5],
        jnp.swapaxes(operands[6], 0, 1),
        *operands[7:],
    )


def fits(ra, cb, chunks, shape, local_width, local_units):
    rem = local_units % LANES
    return (
        ra == 4
        and shape[0] == 2
        and shape[1] % (chunks * 16) == 0
        and local_width % LANES == 0
        and local_width % 32 == 0
        and local_units % 32 == 0
        and 2 * rem + 2 <= LANES
        and local_units >= LANES
        and share_shape(2 * shape[1] // chunks, local_width, cb) is not None
    )


def either(ra, cb, *operands):
    tokens, gate_weight = operands[0], operands[2]
    if fits(ra, cb, CHUNKS, tokens.shape, tokens.shape[2], gate_weight.shape[2]):
        return fused_shards(ra, cb, CHUNKS, *operands)
    return shards(*operands)


def solution(mesh):
    in_specs = (
        P(None, None, "ra"),
        P(None, "ra"),
        P(None, "ra", "cb"),
        P(None, "cb"),
        P(None, "ra", "cb"),
        P(None, "cb"),
        P(None, None, "cb"),
        P(None, "cb"),
        P(None, "cb", "ra"),
        P(None, "ra"),
    )
    out_specs = P(None, None, "ra")
    return jax.shard_map(
        functools.partial(either, mesh.shape["ra"], mesh.shape["cb"]),
        mesh=mesh,
        in_specs=in_specs,
        out_specs=out_specs,
        check_vma=False,
    )
```

profile of v0, /device:TPU:0, one launch (start us, length us, event | category | flops | bytes accessed | tf_op | source)
XLA Modules:
  0.0 82.0 jit_solution(13708562211739060017)
XLA Ops:
  0.0 80.2 %shard_map.100 = bf16[2,128,768]{2,1,0:T(8,128)(2,1)} custom-call(bf16[2,128,768]{2,1,0:T(8,128)(2,1)} %tokens.1, f32[2,768]{1,0:T(2,128)} %norm_gain.1, f32[2,1056,768]{2,1,0:T(8,128)} %bitcast.3, f32[2,1056]{1,0:T(2,128)} %gate_scale.1, f32[2,1056,768]{2,1,0:T(8,128)} %bitcast.4, f32[2,1056]{1,0:T(2,128)} %up_scale.1, f32[3,2,1056]{2,1,0:T(2,128)} %bitcast.5, ...), custom_call_target="tpu_custom_call" | custom-call | tf_op jit(solution)/shard_map/pallas_call | solution.py:510
  80.2 1.8 %copy.12 = bf16[2,128,768]{2,1,0:T(8,128)(2,1)} copy(bf16[2,128,768]{2,1,0:T(8,128)(2,1)} %shard_map.100) | data formatting | bytes 786432
where the time goes:
time: 82.1 us; the launch traced here: 82 us
  Pallas kernels  80.2 us (98%)
  local copies, waits for them, and re-layouts  1.77 us (2%)
    pallas_call x1, Pallas kernels, fused_shards(): pl.pallas_call(functools.partial(fused, chunks, ra, cb), out_shape=jax.Sh...  80.2 us
    unnamed x1, local copies, waits for them, and re-layouts  1.77 us

commit v1 on v0

--- a/solution.py
+++ b/solution.py
@@ -94,29 +94,42 @@
 MESH = pl.DeviceIdType.MESH
 LANES = 128
 CHUNKS = 8
-LAG = dict(enter=0, mix=2, act=3, down=4, fold=6, done=8)
-ORDER = ("done", "mix", "enter", "act", "fold", "down")
-GAP = 8
+PLAN = (
+    ("enter", 0),
+    ("act", 3),
+    ("pair", 5),
+    ("fold", 6),
+    ("mix", 1),
+    ("down", 4),
+    ("done", 6),
+)
+CONVERT = {1: ("out", 0), 3: ("in", 1), 5: ("out", 1)}
 
 
 def fused(
     chunks,
     ra,
     cb,
-    tokens,
-    norm_gain,
+    tokens_hbm,
+    norm_gain_hbm,
     gate_weight,
-    gate_scale,
+    gate_scale_hbm,
     up_weight,
-    up_scale,
-    conv_weight,
-    conv_bias,
+    up_scale_hbm,
+    conv_weight_hbm,
+    conv_bias_hbm,
     down_weight,
-    down_scale,
+    down_scale_hbm,
     out,
     stage_gate,
     stage_up,
     stage_down,
+    norm_gain,
+    gate_scale,
+    up_scale,
+    conv_weight,
+    conv_bias,
+    down_scale,
     in_w,
     out_w,
     state,
@@ -125,24 +138,30 @@
     far_send,
     far_part,
     hidden,
-    down_part,
-    down_recv,
+    down_keep,
+    pair_send,
+    pair_recv,
+    chip_part,
     conv_pad,
     params,
     load_sem,
+    small_sem,
+    token_sem,
     near_s,
     near_r,
     far_s,
     far_r,
     hid_s,
     hid_r,
-    red_s,
-    red_r,
+    pair_s,
+    pair_r,
+    chip_s,
+    chip_r,
     out_s,
     out_r,
 ):
     layers = 2
-    sequences, length, width = tokens.shape
+    sequences, length, width = tokens_hbm.shape
     units = gate_weight.shape[1]
     main = units // LANES * LANES
     rem = units - main
@@ -150,85 +169,125 @@
     step = length // chunks
     rows = sequences * step
     items = layers * chunks
-    share_rows, share_cols = down_recv.shape[2], down_recv.shape[3]
-    col_parts = width // share_cols
+    half = width // 2
+    chips = cb // 2
+    split = main // 2
     me = lax.axis_index("ra")
     mine = lax.axis_index("cb")
+    core = lax.rem(mine, 2)
+    chip = mine // 2
     inner = jnp.logical_and(me >= 1, me <= 2)
     outer = jnp.logical_not(inner)
     own_seq = me - 1
-
-    loads = []
-    for layer in range(layers):
-        for kind, (src, dst) in enumerate(
-            ((gate_weight, stage_gate), (up_weight, stage_up), (down_weight, stage_down))
-        ):
-            loads.append(
-                pltpu.make_async_copy(src.at[layer], dst.at[layer], load_sem.at[layer * 3 + kind])
-            )
-    for load in loads:
-        load.start()
+    my_cols = pl.ds(pl.multiple_of(core * half, LANES), half)
+    other_cols = pl.ds(pl.multiple_of((1 - core) * half, LANES), half)
 
     barrier = pltpu.get_barrier_semaphore()
     for d in range(1, ra):
+        to = lax.rem(me + d, ra)
+
+        @pl.when(jnp.logical_or(inner, jnp.logical_and(to >= 1, to <= 2)))
+        def _():
+            pl.semaphore_signal(barrier, inc=1, device_id={"ra": to}, device_id_type=MESH)
+
+    pl.semaphore_signal(
+        barrier, inc=1, device_id={"cb": 2 * chip + 1 - core}, device_id_type=MESH
+    )
+    for d in range(1, chips):
         pl.semaphore_signal(
-            barrier, inc=1, device_id={"ra": lax.rem(me + d, ra)}, device_id_type=MESH
-        )
-    for d in range(1, cb):
-        pl.semaphore_signal(
-            barrier, inc=1, device_id={"cb": lax.rem(mine + d, cb)}, device_id_type=MESH
-        )
-
-    for c in range(chunks):
+            barrier,
+            inc=1,
+            device_id={"cb": 2 * lax.rem(chip + d, chips) + core},
+            device_id_type=MESH,
+        )
+
+    def token_copy(c, s):
+        return pltpu.make_async_copy(
+            tokens_hbm.at[s, pl.ds(pl.multiple_of(c * step, step), step)],
+            state.at[c, pl.ds(s * step, step)],
+            token_sem.at[c, s],
+        )
+
+    smalls = [
+        pltpu.make_async_copy(src, dst, small_sem.at[i])
+        for i, (src, dst) in enumerate(
+            (
+                (norm_gain_hbm, norm_gain),
+                (gate_scale_hbm, gate_scale),
+                (up_scale_hbm, up_scale),
+                (conv_weight_hbm, conv_weight),
+                (conv_bias_hbm, conv_bias),
+                (down_scale_hbm, down_scale),
+            )
+        )
+    ]
+    pieces = ((0, split), (split, units - split))
+
+    def load(layer, kind, part):
+        src, dst = (
+            (gate_weight, stage_gate),
+            (up_weight, stage_up),
+            (down_weight, stage_down),
+        )[kind]
+        r = pl.ds(*pieces[part])
+        return pltpu.make_async_copy(
+            src.at[layer, r], dst.at[layer, r], load_sem.at[layer * 6 + kind * 2 + part]
+        )
+
+    for s in range(sequences):
+        token_copy(0, s).start()
+    smalls[0].start()
+    for part in range(2):
+        for kind in range(2):
+            load(0, kind, part).start()
+    for copy in smalls[1:]:
+        copy.start()
+    for c in range(1, chunks):
         for s in range(sequences):
-            state[c, s * step : (s + 1) * step, :] = tokens[
-                s, c * step : (c + 1) * step, :
-            ].astype(state.dtype)
-
-    def convert_in(layer):
-        loads[layer * 3].wait()
-        loads[layer * 3 + 1].wait()
-        block = 32
-
-        @pl.loop(0, main // block)
+            token_copy(c, s).start()
+    for part in range(2):
+        load(0, 2, part).start()
+    for kind in range(3):
+        for part in range(2):
+            load(1, kind, part).start()
+
+    block = 32
+
+    def convert_piece(layer, kind, part):
+        load(layer, kind, part).wait()
+        src = (stage_gate, stage_up)[kind]
+        first, stop = part * split, (part + 1) * split
+
+        @pl.loop(first // block, stop // block)
         def _(i):
             r = pl.ds(pl.multiple_of(i * block, block), block)
-            r2 = pl.ds(pl.multiple_of(main + i * block, block), block)
-            in_w[layer, r, :] = stage_gate[layer, r, :].astype(jnp.bfloat16)
-            in_w[layer, r2, :] = stage_up[layer, r, :].astype(jnp.bfloat16)
-
-        first = 2 * main
-        if rem:
-            in_w[layer, first : first + rem, :] = stage_gate[layer, main:, :].astype(jnp.bfloat16)
-            in_w[layer, first + rem : first + 2 * rem, :] = stage_up[layer, main:, :].astype(
-                jnp.bfloat16
-            )
-        in_w[layer, first + 2 * rem :, :] = jnp.zeros((LANES - 2 * rem, width), jnp.bfloat16)
+            r2 = pl.ds(pl.multiple_of(kind * main + i * block, block), block)
+            in_w[layer, r2, :] = src[layer, r, :].astype(jnp.bfloat16)
+
+        if rem and part:
+            first = 2 * main + kind * rem
+            in_w[layer, first : first + rem, :] = src[layer, main:, :].astype(jnp.bfloat16)
+
+    def convert_in(layer):
+        for part in range(2):
+            for kind in range(2):
+                convert_piece(layer, kind, part)
+        first = 2 * main + 2 * rem
+        in_w[layer, first:, :] = jnp.zeros((LANES - 2 * rem, width), jnp.bfloat16)
 
     def convert_out(layer):
-        loads[layer * 3 + 2].wait()
-        block = 32
+        for part in range(2):
+            load(layer, 2, part).wait()
 
         @pl.loop(0, units // block)
         def _(i):
             r = pl.ds(pl.multiple_of(i * block, block), block)
-            out_w[layer, r, :] = stage_down[layer, r, :].astype(jnp.bfloat16)
+            out_w[layer, r, :half] = stage_down[layer, r, other_cols].astype(jnp.bfloat16)
+            out_w[layer, r, half:] = stage_down[layer, r, my_cols].astype(jnp.bfloat16)
 
         pad = out_w.shape[1] - units
         if pad:
             out_w[layer, units:, :] = jnp.zeros((pad, width), jnp.bfloat16)
-
-    for layer in range(layers):
-        lines = [gate_scale[layer : layer + 1, :], up_scale[layer : layer + 1, :]]
-        lines.append(conv_bias[layer : layer + 1, :])
-        lines += [conv_weight[j, layer : layer + 1, :] for j in range(conv_weight.shape[0])]
-        for row, line in enumerate(lines):
-            if rem:
-                zeros = jnp.zeros((1, LANES - rem), jnp.float32)
-                params[layer, row : row + 1, main:] = jnp.concatenate(
-                    [line[:, main:], zeros], axis=1
-                )
-            params[layer, row : row + 1, :main] = line[:, :main]
 
     lane = lax.broadcasted_iota(jnp.int32, (1, LANES), 1)
 
@@ -277,44 +336,61 @@
             device_id_type=MESH,
         )
 
-    def share(p):
-        return (
-            pl.ds(pl.multiple_of(p // col_parts * share_rows, share_rows), share_rows),
-            pl.ds(pl.multiple_of(p % col_parts * share_cols, LANES), share_cols),
-        )
-
-    def red_copy(k, d):
-        to = lax.rem(mine + d, cb)
-        r, c = share(to)
+    def pair_copy(k):
         return pltpu.make_async_remote_copy(
-            src_ref=down_part.at[k, r, c],
-            dst_ref=down_recv.at[k, d - 1],
-            send_sem=red_s.at[k, d - 1],
-            recv_sem=red_r.at[k, d - 1],
-            device_id={"cb": to},
-            device_id_type=MESH,
-        )
-
-    def out_copy(k, d, owner):
-        r, c = share(owner)
+            src_ref=pair_send.at[k],
+            dst_ref=pair_recv.at[k],
+            send_sem=pair_s.at[k],
+            recv_sem=pair_r.at[k],
+            device_id={"cb": 2 * chip + 1 - core},
+            device_id_type=MESH,
+        )
+
+    def chip_copy(k, d):
         return pltpu.make_async_remote_copy(
-            src_ref=state.at[k + chunks, r, c],
-            dst_ref=state.at[k + chunks, r, c],
-            send_sem=out_s.at[k, d - 1],
-            recv_sem=out_r.at[k, d - 1],
-            device_id={"cb": lax.rem(mine + d, cb)},
-            device_id_type=MESH,
-        )
-
-    def enter(k):
+            src_ref=chip_part.at[k, chip],
+            dst_ref=chip_part.at[k, chip],
+            send_sem=chip_s.at[k, d - 1],
+            recv_sem=chip_r.at[k, d - 1],
+            device_id={"cb": 2 * lax.rem(chip + d, chips) + core},
+            device_id_type=MESH,
+        )
+
+    def chip_wait(k, d):
+        return pltpu.make_async_remote_copy(
+            src_ref=chip_part.at[k, chip],
+            dst_ref=chip_part.at[k, lax.rem(chip - d + chips, chips)],
+            send_sem=chip_s.at[k, d - 1],
+            recv_sem=chip_r.at[k, d - 1],
+            device_id={"cb": 2 * lax.rem(chip + d, chips) + core},
+            device_id_type=MESH,
+        )
+
+    def out_copy(k, cols):
+        return pltpu.make_async_remote_copy(
+            src_ref=state.at[k + chunks, :, cols],
+            dst_ref=state.at[k + chunks, :, cols],
+            send_sem=out_s.at[k],
+            recv_sem=out_r.at[k],
+            device_id={"cb": 2 * chip + 1 - core},
+            device_id_type=MESH,
+        )
+
+    def project(k):
         layer = k // chunks
+
+        @pl.when(k < chunks)
+        def _():
+            for s in range(sequences):
+                token_copy(k, s).wait()
+
         values = state[k].astype(jnp.float32)
         squares = jnp.sum(values * values, axis=1, keepdims=True)
         gain = norm_gain[pl.ds(layer, 1), :]
         scaled = (values * gain).astype(jnp.bfloat16)
-        block = 512
-        for start in range(0, 2 * main, block):
-            stop = min(start + block, 2 * main)
+        cols = 512
+        for start in range(0, 2 * main, cols):
+            stop = min(start + cols, 2 * main)
             own_part[k, :, start:stop] = lax.dot_general(
                 scaled,
                 in_w[layer, start:stop, :],
@@ -329,6 +405,11 @@
         )
         own_part[k, :, 2 * main :] = put_squares(tile, squares).astype(jnp.bfloat16)
 
+    def enter(k):
+        @pl.when(k > 0)
+        def _():
+            project(k)
+
         @pl.when(outer)
         def _():
             near_copy(k, True).start()
@@ -381,9 +462,9 @@
             value = conv / (1.0 + jnp.exp(-conv)) * (up * inverse_rms * param(1))
             hidden[k, r, start:stop] = value.astype(jnp.bfloat16)
 
-        block = 256
-        for start in range(0, main, block):
-            stop = min(start + block, main)
+        cols = 256
+        for start in range(0, main, cols):
+            stop = min(start + cols, main)
             piece(total(start, stop), total(main + start, main + stop), start, stop)
         if rem:
             piece(tile, pltpu.roll(tile, LANES - rem, axis=1), main, main + LANES)
@@ -398,44 +479,67 @@
             def _():
                 hid_copy(k, 1, seq).wait_recv()
 
-        down_part[k] = jnp.dot(
-            hidden[k], out_w[layer], preferred_element_type=jnp.float32
-        ).astype(down_part.dtype)
-        for d in range(1, cb):
-            red_copy(k, d).start()
+        value = jnp.dot(hidden[k], out_w[layer], preferred_element_type=jnp.float32)
+        pair_send[k] = value[:, :half].astype(jnp.bfloat16)
+        down_keep[k] = value[:, half:]
+        pair_copy(k).start()
+
+    def pair(k):
+        pair_copy(k).wait_recv()
+        chip_part[k, chip] = (down_keep[k] + pair_recv[k].astype(jnp.float32)).astype(jnp.bfloat16)
+        for d in range(1, chips):
+            chip_copy(k, d).start()
 
     def fold(k):
         layer = k // chunks
-        r, c = share(mine)
-        total = down_part[k, r, c].astype(jnp.float32)
-        for d in range(1, cb):
-            red_copy(k, d).wait_recv()
-            total = total + down_recv[k, d - 1].astype(jnp.float32)
-        kept = residual_keep * state[k, r, c].astype(jnp.float32)
-        state[k + chunks, r, c] = (
-            (kept + total * down_scale[pl.ds(layer, 1), c])
-            .astype(jnp.bfloat16)
-            .astype(state.dtype)
-        )
-        for d in range(1, cb):
-            out_copy(k, d, mine).start()
+        for d in range(1, chips):
+            chip_wait(k, d).wait_recv()
+        total = chip_part[k, 0].astype(jnp.float32)
+        for g in range(1, chips):
+            total = total + chip_part[k, g].astype(jnp.float32)
+        kept = residual_keep * state[k, :, my_cols].astype(jnp.float32)
+        scale = down_scale[pl.ds(layer, 1), my_cols]
+        state[k + chunks, :, my_cols] = (kept + total * scale).astype(jnp.bfloat16)
+        out_copy(k, my_cols).start()
 
     def done(k):
-        for d in range(1, cb):
-            out_copy(k, d, lax.rem(mine - d + cb, cb)).wait_recv()
-
+        out_copy(k, other_cols).wait_recv()
+
+        @pl.when(k >= chunks)
+        def _():
+            for s in range(sequences):
+                c = pl.ds(pl.multiple_of((k - chunks) * step, step), step)
+                out[s, c, :] = state[k + chunks, s * step : (s + 1) * step, :]
+
+    smalls[0].wait()
     convert_in(0)
-    pl.semaphore_wait(barrier, ra - 1 + cb - 1)
-
-    works = dict(enter=enter, mix=mix, act=act, down=down, fold=fold, done=done)
-
-    @pl.loop(0, GAP + chunks + max(LAG.values()))
+    project(0)
+    pl.semaphore_wait(barrier, jnp.where(inner, ra - 1, ra - 2) + chips)
+
+    works = dict(
+        enter=enter, mix=mix, act=act, down=down, pair=pair, fold=fold, done=done
+    )
+
+    def prepare():
+        for copy in smalls[1:]:
+            copy.wait()
+        for layer in range(layers):
+            lines = [gate_scale[layer : layer + 1, :], up_scale[layer : layer + 1, :]]
+            lines.append(conv_bias[layer : layer + 1, :])
+            lines += [conv_weight[j, layer : layer + 1, :] for j in range(conv_weight.shape[0])]
+            for row, line in enumerate(lines):
+                if rem:
+                    zeros = jnp.zeros((1, LANES - rem), jnp.float32)
+                    params[layer, row : row + 1, main:] = jnp.concatenate(
+                        [line[:, main:], zeros], axis=1
+                    )
+                params[layer, row : row + 1, :main] = line[:, :main]
+
+    @pl.loop(0, items + max(lag for _, lag in PLAN))
     def _(slot):
-        for name in ORDER:
-            place = slot - LAG[name]
-            late = place >= GAP
-            item = jnp.where(late, place - GAP + chunks, place)
-            good = jnp.logical_and(item >= 0, item < jnp.where(late, items, chunks))
+        for name, lag in PLAN:
+            item = slot - lag
+            good = jnp.logical_and(item >= 0, item < items)
             if name in ("mix", "act"):
                 good = jnp.logical_and(good, inner)
 
@@ -447,21 +551,13 @@
 
                 @pl.when(slot == 0)
                 def _():
-                    convert_out(0)
-
-                @pl.when(slot == 1)
-                def _():
-                    convert_in(1)
-
-                @pl.when(slot == 2)
-                def _():
-                    convert_out(1)
-
-    for c in range(chunks):
-        for s in range(sequences):
-            out[s, c * step : (c + 1) * step, :] = state[
-                items + c, s * step : (s + 1) * step, :
-            ].astype(jnp.bfloat16)
+                    prepare()
+
+                for at, (kind, layer) in CONVERT.items():
+
+                    @pl.when(slot == at)
+                    def _():
+                        (convert_in if kind == "in" else convert_out)(layer)
 
     @pl.loop(0, items)
     def _(k):
@@ -476,19 +572,10 @@
             for d in range(1, ra):
                 hid_copy(k, d, own_seq).wait_send()
 
-        for d in range(1, cb):
-            red_copy(k, d).wait_send()
-            out_copy(k, d, mine).wait_send()
-
-
-def share_shape(rows, width, parts):
-    for tile, dtype in ((16, jnp.bfloat16), (8, jnp.float32)):
-        for col_parts in range(1, parts + 1):
-            if parts % col_parts or width % (col_parts * LANES):
-                continue
-            if rows % (parts // col_parts * tile) == 0:
-                return (rows * col_parts // parts, width // col_parts), dtype
-    return None
+        pair_copy(k).wait_send()
+        for d in range(1, chips):
+            chip_copy(k, d).wait_send()
+        out_copy(k, my_cols).wait_send()
 
 
 def fused_shards(ra, cb, chunks, *operands):
@@ -502,43 +589,56 @@
     step = length // chunks
     rows = sequences * step
     items = layers * chunks
-    part, part_type = share_shape(rows, width, cb)
-    vmem = pl.BlockSpec(memory_space=pltpu.VMEM)
+    half = width // 2
+    chips = cb // 2
+    taps = operands[6].shape[1]
     hbm = pl.BlockSpec(memory_space=pl.ANY)
     dma = pltpu.SemaphoreType.DMA
     bf16, f32 = jnp.bfloat16, jnp.float32
     return pl.pallas_call(
         functools.partial(fused, chunks, ra, cb),
-        out_shape=jax.ShapeDtypeStruct(tokens.shape, tokens.dtype),
-        in_specs=[vmem, vmem, hbm, vmem, hbm, vmem, vmem, vmem, hbm, vmem],
-        out_specs=vmem,
+        out_shape=pltpu.VMEM(tokens.shape, tokens.dtype),
+        in_specs=[hbm] * 10,
+        out_specs=pl.BlockSpec(memory_space=pltpu.VMEM),
         scratch_shapes=[
             pltpu.VMEM((layers, units, width), f32),
             pltpu.VMEM((layers, units, width), f32),
             pltpu.VMEM((layers, units, width), f32),
+            pltpu.VMEM((layers, width), f32),
+            pltpu.VMEM((layers, units), f32),
+            pltpu.VMEM((layers, units), f32),
+            pltpu.VMEM((taps, layers, units), f32),
+            pltpu.VMEM((layers, units), f32),
+            pltpu.VMEM((layers, width), f32),
             pltpu.VMEM((layers, total_cols, width), bf16),
             pltpu.VMEM((layers, padded, width), bf16),
-            pltpu.VMEM((items + chunks, rows, width), part_type),
+            pltpu.VMEM((items + chunks, rows, width), bf16),
             pltpu.VMEM((items, rows, total_cols), bf16),
             pltpu.VMEM((items, rows, total_cols), bf16),
             pltpu.VMEM((items, step, total_cols), bf16),
             pltpu.VMEM((items, step, total_cols), bf16),
             pltpu.VMEM((items, rows, padded), bf16),
-            pltpu.VMEM((items, rows, width), part_type),
-            pltpu.VMEM((items, cb - 1) + part, part_type),
+            pltpu.VMEM((items, rows, half), f32),
+            pltpu.VMEM((items, rows, half), bf16),
+            pltpu.VMEM((items, rows, half), bf16),
+            pltpu.VMEM((items, chips, rows, half), bf16),
             pltpu.VMEM((8 + step, padded), f32),
-            pltpu.VMEM((layers, 3 + operands[6].shape[1], padded), f32),
-            dma((layers * 3,)),
+            pltpu.VMEM((layers, 3 + taps, padded), f32),
+            dma((layers * 6,)),
+            dma((6,)),
+            dma((chunks, sequences)),
             dma((items, sequences)),
             dma((items, sequences)),
             dma((items,)),
             dma((items,)),
             dma((items, ra - 1)),
             dma((items, sequences)),
-            dma((items, cb - 1)),
-            dma((items, cb - 1)),
-            dma((items, cb - 1)),
-            dma((items, cb - 1)),
+            dma((items,)),
+            dma((items,)),
+            dma((items, chips - 1)),
+            dma((items, chips - 1)),
+            dma((items,)),
+            dma((items,)),
         ],
         compiler_params=pltpu.CompilerParams(
             collective_id=0, has_side_effects=True, vmem_limit_bytes=60 * 1024 * 1024
@@ -558,14 +658,14 @@
     rem = local_units % LANES
     return (
         ra == 4
+        and cb % 2 == 0
+        and cb >= 4
         and shape[0] == 2
         and shape[1] % (chunks * 16) == 0
-        and local_width % LANES == 0
-        and local_width % 32 == 0
+        and local_width % (2 * LANES) == 0
         and local_units % 32 == 0
         and 2 * rem + 2 <= LANES
-        and local_units >= LANES
-        and share_shape(2 * shape[1] // chunks, local_width, cb) is not None
+        and local_units >= 2 * LANES
     )
 
 

time: 82.1 us -> 76.2 us (0.928)
  Pallas kernels: 80.2 us -> 75.3 us
  local copies, waits for them, and re-layouts: 1.77 us -> 0.75 us
    pallas_call x1, Pallas kernels: 80.2 us -> 75.3 us  [fused_shards(): pl.pallas_call(functools.partial(fused, chunks, ra, cb), out_shape=pltpu....]
    unnamed x1, local copies, waits for them, and re-layouts: 1.77 us -> 0.75 us
where the time goes in v1:
time: 76.2 us; the launch traced here: 76.1 us
  Pallas kernels  75.3 us (99%)
    pallas_call x1, Pallas kernels, fused_shards(): pl.pallas_call(functools.partial(fused, chunks, ra, cb), out_shape=pltpu....  75.3 us

profile of v1, /device:TPU:0, one launch (start us, length us, event | category | flops | bytes accessed | tf_op | source)
XLA Modules:
  0.0 76.1 jit_solution(10093613599331723996)
XLA Ops:
  0.0 75.3 %shard_map.100 = bf16[2,128,768]{2,1,0:T(8,128)(2,1)S(1)} custom-call(bf16[2,128,768]{2,1,0:T(8,128)(2,1)} %tokens_hbm.1, f32[2,768]{1,0:T(2,128)} %norm_gain_hbm.1, f32[2,1056,768]{2,1,0:T(8,128)} %bitcast.3, f32[2,1056]{1,0:T(2,128)} %gate_scale_hbm.1, f32[2,1056,768]{2,1,0:T(8,128)} %bitcast.4, f32[2,1056]{1,0:T(2,128)} %up_scale_hbm.1, ...), custom_call_target="tpu_custom_call" | custom-call | tf_op jit(solution)/shard_map/pallas_call | solution.py:598
  75.3 0.7 copy.12

commit v2 on v1

--- a/solution.py
+++ b/solution.py
@@ -94,15 +94,7 @@
 MESH = pl.DeviceIdType.MESH
 LANES = 128
 CHUNKS = 8
-PLAN = (
-    ("enter", 0),
-    ("act", 3),
-    ("pair", 5),
-    ("fold", 6),
-    ("mix", 1),
-    ("down", 4),
-    ("done", 6),
-)
+PLAN = (('done', 8), ('act', 3), ('enter', 0), ('pair', 5), ('fold', 7), ('mix', 1), ('down', 4))
 CONVERT = {1: ("out", 0), 3: ("in", 1), 5: ("out", 1)}
 
 
@@ -245,11 +237,6 @@
     for c in range(1, chunks):
         for s in range(sequences):
             token_copy(c, s).start()
-    for part in range(2):
-        load(0, 2, part).start()
-    for kind in range(3):
-        for part in range(2):
-            load(1, kind, part).start()
 
     block = 32
 
@@ -513,6 +500,11 @@
 
     smalls[0].wait()
     convert_in(0)
+    for part in range(2):
+        load(0, 2, part).start()
+    for kind in range(3):
+        for part in range(2):
+            load(1, kind, part).start()
     project(0)
     pl.semaphore_wait(barrier, jnp.where(inner, ra - 1, ra - 2) + chips)
 

time: 76.2 us -> 74.8 us (0.982)
  Pallas kernels: 75.3 us -> 73.9 us
    pallas_call x1, Pallas kernels: 75.3 us -> 73.9 us  [fused_shards(): pl.pallas_call(functools.partial(fused, chunks, ra, cb), out_shape=pltpu....]
where the time goes in v2:
time: 74.8 us; the launch traced here: 74.6 us
  Pallas kernels  73.9 us (99%)
  local copies, waits for them, and re-layouts  0.75 us (1%)
    pallas_call x1, Pallas kernels, fused_shards(): pl.pallas_call(functools.partial(fused, chunks, ra, cb), out_shape=pltpu....  73.9 us

profile of v2, /device:TPU:0, one launch (start us, length us, event | category | flops | bytes accessed | tf_op | source)
XLA Modules:
  0.0 74.6 jit_solution(12890573161580864318)
XLA Ops:
  0.0 73.9 %shard_map.100 = bf16[2,128,768]{2,1,0:T(8,128)(2,1)S(1)} custom-call(bf16[2,128,768]{2,1,0:T(8,128)(2,1)} %tokens_hbm.1, f32[2,768]{1,0:T(2,128)} %norm_gain_hbm.1, f32[2,1056,768]{2,1,0:T(8,128)} %bitcast.3, f32[2,1056]{1,0:T(2,128)} %gate_scale_hbm.1, f32[2,1056,768]{2,1,0:T(8,128)} %bitcast.4, f32[2,1056]{1,0:T(2,128)} %up_scale_hbm.1, ...), custom_call_target="tpu_custom_call" | custom-call | tf_op jit(solution)/shard_map/pallas_call | solution.py:590
  73.9 0.7 %copy.12 = bf16[2,128,768]{2,1,0:T(8,128)(2,1)} copy(bf16[2,128,768]{2,1,0:T(8,128)(2,1)S(1)} %shard_map.100) | data formatting | bytes 786432

commit v3 on v2

--- a/solution.py
+++ b/solution.py
@@ -94,6 +94,7 @@
 MESH = pl.DeviceIdType.MESH
 LANES = 128
 CHUNKS = 8
+GROUPS = 2
 PLAN = (('done', 8), ('act', 3), ('enter', 0), ('pair', 5), ('fold', 7), ('mix', 1), ('down', 4))
 CONVERT = {1: ("out", 0), 3: ("in", 1), 5: ("out", 1)}
 
@@ -163,7 +164,12 @@
     items = layers * chunks
     half = width // 2
     chips = cb // 2
-    split = main // 2
+    size = main // GROUPS
+    lines_in = [(0, 2 * size + LANES)]
+    lines_hid = [(0, size + (LANES if rem else 0))]
+    for g in range(1, GROUPS):
+        lines_in.append((sum(lines_in[-1]), 2 * size))
+        lines_hid.append((sum(lines_hid[-1]), size))
     me = lax.axis_index("ra")
     mine = lax.axis_index("cb")
     core = lax.rem(mine, 2)
@@ -213,23 +219,25 @@
             )
         )
     ]
-    pieces = ((0, split), (split, units - split))
+    pieces = [(g * size, size) for g in range(GROUPS)] + ([(main, rem)] if rem else [])
+    early = [0] + list(range(GROUPS, len(pieces))) + list(range(1, GROUPS))
 
     def load(layer, kind, part):
-        src, dst = (
-            (gate_weight, stage_gate),
-            (up_weight, stage_up),
-            (down_weight, stage_down),
-        )[kind]
+        src, dst = ((gate_weight, stage_gate), (up_weight, stage_up))[kind]
         r = pl.ds(*pieces[part])
         return pltpu.make_async_copy(
-            src.at[layer, r], dst.at[layer, r], load_sem.at[layer * 6 + kind * 2 + part]
+            src.at[layer, r], dst.at[layer, r], load_sem.at[layer, kind * len(pieces) + part]
+        )
+
+    def load_out(layer):
+        return pltpu.make_async_copy(
+            down_weight.at[layer], stage_down.at[layer], load_sem.at[layer, 2 * len(pieces)]
         )
 
     for s in range(sequences):
         token_copy(0, s).start()
     smalls[0].start()
-    for part in range(2):
+    for part in early:
         for kind in range(2):
             load(0, kind, part).start()
     for copy in smalls[1:]:
@@ -243,38 +251,51 @@
     def convert_piece(layer, kind, part):
         load(layer, kind, part).wait()
         src = (stage_gate, stage_up)[kind]
-        first, stop = part * split, (part + 1) * split
-
-        @pl.loop(first // block, stop // block)
-        def _(i):
-            r = pl.ds(pl.multiple_of(i * block, block), block)
-            r2 = pl.ds(pl.multiple_of(kind * main + i * block, block), block)
-            in_w[layer, r2, :] = src[layer, r, :].astype(jnp.bfloat16)
-
-        if rem and part:
-            first = 2 * main + kind * rem
+        if part < GROUPS:
+            shift = lines_in[part][0] + kind * size - part * size
+
+            @pl.loop(part * size // block, (part + 1) * size // block)
+            def _(i):
+                r = pl.ds(pl.multiple_of(i * block, block), block)
+                r2 = pl.ds(pl.multiple_of(shift + i * block, block), block)
+                in_w[layer, r2, :] = src[layer, r, :].astype(jnp.bfloat16)
+
+        else:
+            first = 2 * size + kind * rem
             in_w[layer, first : first + rem, :] = src[layer, main:, :].astype(jnp.bfloat16)
 
-    def convert_in(layer):
-        for part in range(2):
+    def convert_group(layer, g):
+        for part in [g] + (list(range(GROUPS, len(pieces))) if g == 0 else []):
             for kind in range(2):
                 convert_piece(layer, kind, part)
-        first = 2 * main + 2 * rem
-        in_w[layer, first:, :] = jnp.zeros((LANES - 2 * rem, width), jnp.bfloat16)
+        if g == 0:
+            first = 2 * size + 2 * rem
+            in_w[layer, first : 2 * size + LANES, :] = jnp.zeros(
+                (LANES - 2 * rem, width), jnp.bfloat16
+            )
+
+    def convert_in(layer):
+        for g in range(GROUPS):
+            convert_group(layer, g)
 
     def convert_out(layer):
-        for part in range(2):
-            load(layer, 2, part).wait()
-
-        @pl.loop(0, units // block)
-        def _(i):
-            r = pl.ds(pl.multiple_of(i * block, block), block)
-            out_w[layer, r, :half] = stage_down[layer, r, other_cols].astype(jnp.bfloat16)
-            out_w[layer, r, half:] = stage_down[layer, r, my_cols].astype(jnp.bfloat16)
-
-        pad = out_w.shape[1] - units
-        if pad:
-            out_w[layer, units:, :] = jnp.zeros((pad, width), jnp.bfloat16)
+        load_out(layer).wait()
+
+        def rows_to(first, shift, count):
+            @pl.loop(first // block, (first + count) // block)
+            def _(i):
+                r = pl.ds(pl.multiple_of(i * block, block), block)
+                r2 = pl.ds(pl.multiple_of(shift + i * block, block), block)
+                out_w[layer, r2, :half] = stage_down[layer, r, other_cols].astype(jnp.bfloat16)
+                out_w[layer, r2, half:] = stage_down[layer, r, my_cols].astype(jnp.bfloat16)
+
+        for g in range(GROUPS):
+            rows_to(g * size, lines_hid[g][0] - g * size, size)
+        if rem:
+            rows_to(main, size - main, rem)
+            out_w[layer, size + rem : size + LANES, :] = jnp.zeros(
+                (LANES - rem, width), jnp.bfloat16
+            )
 
     lane = lax.broadcasted_iota(jnp.int32, (1, LANES), 1)
 
@@ -287,25 +308,25 @@
         keep = jnp.logical_and(lane >= 2 * rem, lane < 2 * rem + 2)
         return jnp.sum(jnp.where(keep, tile, 0.0), axis=1, keepdims=True)
 
-    def near_copy(k, first):
+    def near_copy(k, first, g):
         to = jnp.where(me == 0, 1, 2)
         passed = jnp.where(me < 2, 1, 0)
         r = hid_rows(passed if first else 1 - passed)
         return pltpu.make_async_remote_copy(
-            src_ref=own_part.at[k, r],
-            dst_ref=near_part.at[k, r],
-            send_sem=near_s.at[k, int(first)],
-            recv_sem=near_r.at[k, int(first)],
+            src_ref=own_part.at[k, r, pl.ds(*lines_in[g])],
+            dst_ref=near_part.at[k, r, pl.ds(*lines_in[g])],
+            send_sem=near_s.at[k, 2 * g + int(first)],
+            recv_sem=near_r.at[k, 2 * g + int(first)],
             device_id={"ra": to},
             device_id_type=MESH,
         )
 
-    def far_copy(k):
+    def far_copy(k, g):
         return pltpu.make_async_remote_copy(
-            src_ref=far_send.at[k],
-            dst_ref=far_part.at[k],
-            send_sem=far_s.at[k],
-            recv_sem=far_r.at[k],
+            src_ref=far_send.at[k, :, pl.ds(*lines_in[g])],
+            dst_ref=far_part.at[k, :, pl.ds(*lines_in[g])],
+            send_sem=far_s.at[k, g],
+            recv_sem=far_r.at[k, g],
             device_id={"ra": 3 - me},
             device_id_type=MESH,
         )
@@ -313,12 +334,12 @@
     def hid_rows(seq):
         return pl.ds(pl.multiple_of(seq * step, step), step)
 
-    def hid_copy(k, d, seq):
+    def hid_copy(k, d, seq, g):
         return pltpu.make_async_remote_copy(
-            src_ref=hidden.at[k, hid_rows(seq)],
-            dst_ref=hidden.at[k, hid_rows(seq)],
-            send_sem=hid_s.at[k, d - 1],
-            recv_sem=hid_r.at[k, seq],
+            src_ref=hidden.at[k, hid_rows(seq), pl.ds(*lines_hid[g])],
+            dst_ref=hidden.at[k, hid_rows(seq), pl.ds(*lines_hid[g])],
+            send_sem=hid_s.at[k, (d - 1) * GROUPS + g],
+            recv_sem=hid_r.at[k, seq * GROUPS + g],
             device_id={"ra": lax.rem(me + d, ra)},
             device_id_type=MESH,
         )
@@ -363,7 +384,7 @@
             device_id_type=MESH,
         )
 
-    def project(k):
+    def scaled_rows(k):
         layer = k // chunks
 
         @pl.when(k < chunks)
@@ -374,51 +395,67 @@
         values = state[k].astype(jnp.float32)
         squares = jnp.sum(values * values, axis=1, keepdims=True)
         gain = norm_gain[pl.ds(layer, 1), :]
-        scaled = (values * gain).astype(jnp.bfloat16)
+        return (values * gain).astype(jnp.bfloat16), squares
+
+    def project(k, scaled, squares, g):
+        layer = k // chunks
+        begin, count = lines_in[g]
         cols = 512
-        for start in range(0, 2 * main, cols):
-            stop = min(start + cols, 2 * main)
-            own_part[k, :, start:stop] = lax.dot_general(
+
+        def product(start, stop):
+            return lax.dot_general(
                 scaled,
                 in_w[layer, start:stop, :],
                 (((1,), (1,)), ((), ())),
                 preferred_element_type=jnp.float32,
-            ).astype(jnp.bfloat16)
-        tile = lax.dot_general(
-            scaled,
-            in_w[layer, 2 * main :, :],
-            (((1,), (1,)), ((), ())),
-            preferred_element_type=jnp.float32,
-        )
-        own_part[k, :, 2 * main :] = put_squares(tile, squares).astype(jnp.bfloat16)
+            )
+
+        plain = begin + 2 * size
+        for start in range(begin, plain, cols):
+            stop = min(start + cols, plain)
+            own_part[k, :, start:stop] = product(start, stop).astype(jnp.bfloat16)
+        if g == 0:
+            tile = put_squares(product(plain, plain + LANES), squares)
+            own_part[k, :, plain : plain + LANES] = tile.astype(jnp.bfloat16)
+
+    def send_near(k, g, which=(True, False)):
+        @pl.when(outer)
+        def _():
+            for first in which:
+                near_copy(k, first, g).start()
 
     def enter(k):
         @pl.when(k > 0)
         def _():
-            project(k)
-
-        @pl.when(outer)
-        def _():
-            near_copy(k, True).start()
-            near_copy(k, False).start()
+            scaled, squares = scaled_rows(k)
+            for g in range(GROUPS):
+                project(k, scaled, squares, g)
+                send_near(k, g, (True,))
+            for g in range(GROUPS):
+                send_near(k, g, (False,))
 
     def mix(k):
-        near_copy(k, True).wait_recv()
         r = hid_rows(1 - own_seq)
-        both = own_part[k, r, : 2 * main].astype(jnp.float32) + near_part[
-            k, r, : 2 * main
-        ].astype(jnp.float32)
-        far_send[k, :, : 2 * main] = both.astype(jnp.bfloat16)
-        tile = own_part[k, r, 2 * main :].astype(jnp.float32) + near_part[k, r, 2 * main :].astype(
-            jnp.float32
-        )
-        far_send[k, :, 2 * main :] = put_squares(tile, get_squares(tile)).astype(jnp.bfloat16)
-        far_copy(k).start()
+        for g in range(GROUPS):
+            near_copy(k, True, g).wait_recv()
+            begin = lines_in[g][0]
+            plain = begin + 2 * size
+
+            def both(start, stop):
+                return own_part[k, r, start:stop].astype(jnp.float32) + near_part[
+                    k, r, start:stop
+                ].astype(jnp.float32)
+
+            far_send[k, :, begin:plain] = both(begin, plain).astype(jnp.bfloat16)
+            if g == 0:
+                tile = both(plain, plain + LANES)
+                far_send[k, :, plain : plain + LANES] = put_squares(
+                    tile, get_squares(tile)
+                ).astype(jnp.bfloat16)
+            far_copy(k, g).start()
 
     def act(k):
         layer = k // chunks
-        near_copy(k, False).wait_recv()
-        far_copy(k).wait_recv()
         r = hid_rows(own_seq)
 
         def total(start, stop):
@@ -428,14 +465,11 @@
                 + far_part[k, :, start:stop].astype(jnp.float32)
             )
 
-        tile = total(2 * main, total_cols)
-        inverse_rms = lax.rsqrt(get_squares(tile) / (width * ra) + eps)
-
         @pl.when(k % chunks == 0)
         def _():
             conv_pad[0:8, :] = jnp.zeros((8, conv_pad.shape[1]), jnp.float32)
 
-        def piece(gate, up, start, stop):
+        def piece(inverse_rms, gate, up, start, stop):
             def param(row):
                 return params[layer, row : row + 1, start:stop]
 
@@ -450,13 +484,24 @@
             hidden[k, r, start:stop] = value.astype(jnp.bfloat16)
 
         cols = 256
-        for start in range(0, main, cols):
-            stop = min(start + cols, main)
-            piece(total(start, stop), total(main + start, main + stop), start, stop)
-        if rem:
-            piece(tile, pltpu.roll(tile, LANES - rem, axis=1), main, main + LANES)
-        for d in (2, 1, 3):
-            hid_copy(k, d, own_seq).start()
+        inverse_rms = None
+        for g in range(GROUPS):
+            near_copy(k, False, g).wait_recv()
+            far_copy(k, g).wait_recv()
+            begin, to = lines_in[g][0], lines_hid[g][0]
+            if g == 0:
+                tile = total(2 * size, 2 * size + LANES)
+                inverse_rms = lax.rsqrt(get_squares(tile) / (width * ra) + eps)
+                if rem:
+                    up = pltpu.roll(tile, LANES - rem, axis=1)
+                    piece(inverse_rms, tile, up, size, size + LANES)
+            for start in range(0, size, cols):
+                stop = min(start + cols, size)
+                gate = total(begin + start, begin + stop)
+                up = total(begin + size + start, begin + size + stop)
+                piece(inverse_rms, gate, up, to + start, to + stop)
+            for d in (2, 1, 3):
+                hid_copy(k, d, own_seq, g).start()
 
     def down(k):
         layer = k // chunks
@@ -464,7 +509,8 @@
 
             @pl.when(jnp.logical_not(jnp.logical_and(inner, own_seq == seq)))
             def _():
-                hid_copy(k, 1, seq).wait_recv()
+                for g in range(GROUPS):
+                    hid_copy(k, 1, seq, g).wait_recv()
 
         value = jnp.dot(hidden[k], out_w[layer], preferred_element_type=jnp.float32)
         pair_send[k] = value[:, :half].astype(jnp.bfloat16)
@@ -499,14 +545,19 @@
                 out[s, c, :] = state[k + chunks, s * step : (s + 1) * step, :]
 
     smalls[0].wait()
-    convert_in(0)
-    for part in range(2):
-        load(0, 2, part).start()
-    for kind in range(3):
-        for part in range(2):
-            load(1, kind, part).start()
-    project(0)
-    pl.semaphore_wait(barrier, jnp.where(inner, ra - 1, ra - 2) + chips)
+    first_scaled, first_squares = scaled_rows(0)
+    for g in range(GROUPS):
+        convert_group(0, g)
+        if g == GROUPS - 1:
+            load_out(0).start()
+            for part in early:
+                for kind in range(2):
+                    load(1, kind, part).start()
+            load_out(1).start()
+        project(0, first_scaled, first_squares, g)
+        if g == 0:
+            pl.semaphore_wait(barrier, jnp.where(inner, ra - 1, ra - 2) + chips)
+        send_near(0, g)
 
     works = dict(
         enter=enter, mix=mix, act=act, down=down, pair=pair, fold=fold, done=done
@@ -522,10 +573,14 @@
             for row, line in enumerate(lines):
                 if rem:
                     zeros = jnp.zeros((1, LANES - rem), jnp.float32)
-                    params[layer, row : row + 1, main:] = jnp.concatenate(
+                    params[layer, row : row + 1, size : size + LANES] = jnp.concatenate(
                         [line[:, main:], zeros], axis=1
                     )
-                params[layer, row : row + 1, :main] = line[:, :main]
+                for g in range(GROUPS):
+                    to = lines_hid[g][0]
+                    params[layer, row : row + 1, to : to + size] = line[
+                        :, g * size : (g + 1) * size
+                    ]
 
     @pl.loop(0, items + max(lag for _, lag in PLAN))
     def _(slot):
@@ -555,14 +610,16 @@
     def _(k):
         @pl.when(outer)
         def _():
-            near_copy(k, True).wait_send()
-            near_copy(k, False).wait_send()
+            for g in range(GROUPS):
+                near_copy(k, True, g).wait_send()
+                near_copy(k, False, g).wait_send()
 
         @pl.when(inner)
         def _():
-            far_copy(k).wait_send()
-            for d in range(1, ra):
-                hid_copy(k, d, own_seq).wait_send()
+            for g in range(GROUPS):
+                far_copy(k, g).wait_send()
+                for d in range(1, ra):
+                    hid_copy(k, d, own_seq, g).wait_send()
 
         pair_copy(k).wait_send()
         for d in range(1, chips):
@@ -616,15 +673,15 @@
             pltpu.VMEM((items, chips, rows, half), bf16),
             pltpu.VMEM((8 + step, padded), f32),
             pltpu.VMEM((layers, 3 + taps, padded), f32),
-            dma((layers * 6,)),
+            dma((layers, 2 * GROUPS + 3)),
             dma((6,)),
             dma((chunks, sequences)),
-            dma((items, sequences)),
-            dma((items, sequences)),
-            dma((items,)),
-            dma((items,)),
-            dma((items, ra - 1)),
-            dma((items, sequences)),
+            dma((items, 2 * GROUPS)),
+            dma((items, 2 * GROUPS)),
+            dma((items, GROUPS)),
+            dma((items, GROUPS)),
+            dma((items, (ra - 1) * GROUPS)),
+            dma((items, sequences * GROUPS)),
             dma((items,)),
             dma((items,)),
             dma((items, chips - 1)),
@@ -657,7 +714,8 @@
         and local_width % (2 * LANES) == 0
         and local_units % 32 == 0
         and 2 * rem + 2 <= LANES
-        and local_units >= 2 * LANES
+        and local_units >= LANES * GROUPS
+        and local_units // LANES % GROUPS == 0
     )
 
 

time: 74.8 us -> 74.4 us (level)
  no operation moved by 1% of the time
where the time goes in v3:
time: 74.4 us; the launch traced here: 74 us
  Pallas kernels  73.2 us (98%)
  local copies, waits for them, and re-layouts  0.75 us (1%)
    pallas_call x1, Pallas kernels, fused_shards(): pl.pallas_call(functools.partial(fused, chunks, ra, cb), out_shape=pltpu....  73.2 us

profile of v3, /device:TPU:0, one launch (start us, length us, event | category | flops | bytes accessed | tf_op | source)
XLA Modules:
  0.0 74.0 jit_solution(125337456022818527)
XLA Ops:
  0.0 73.2 %shard_map.100 = bf16[2,128,768]{2,1,0:T(8,128)(2,1)S(1)} custom-call(bf16[2,128,768]{2,1,0:T(8,128)(2,1)} %tokens_hbm.1, f32[2,768]{1,0:T(2,128)} %norm_gain_hbm.1, f32[2,1056,768]{2,1,0:T(8,128)} %bitcast.3, f32[2,1056]{1,0:T(2,128)} %gate_scale_hbm.1, f32[2,1056,768]{2,1,0:T(8,128)} %bitcast.4, f32[2,1056]{1,0:T(2,128)} %up_scale_hbm.1, ...), custom_call_target="tpu_custom_call" | custom-call | tf_op jit(solution)/shard_map/pallas_call | solution.py:647
  73.2 0.7 %copy.12 = bf16[2,128,768]{2,1,0:T(8,128)(2,1)} copy(bf16[2,128,768]{2,1,0:T(8,128)(2,1)S(1)} %shard_map.100) | data formatting | bytes 786432

commit v4 on v3

--- a/solution.py
+++ b/solution.py
@@ -95,7 +95,16 @@
 LANES = 128
 CHUNKS = 8
 GROUPS = 2
-PLAN = (('done', 8), ('act', 3), ('enter', 0), ('pair', 5), ('fold', 7), ('mix', 1), ('down', 4))
+PLAN = (
+    ("done", 8),
+    ("act", 3),
+    ("fold", 7),
+    ("enter", 0),
+    ("mix", 1),
+    ("pair", 5),
+    ("down", 4),
+)
+WINDOW = dict(near=6, far=5, hid=6, pair=5, chip=8, out=4)
 CONVERT = {1: ("out", 0), 3: ("in", 1), 5: ("out", 1)}
 
 
@@ -131,10 +140,12 @@
     far_send,
     far_part,
     hidden,
+    hid_rem,
     down_keep,
     pair_send,
     pair_recv,
     chip_part,
+    rows_of,
     conv_pad,
     params,
     load_sem,
@@ -146,6 +157,8 @@
     far_r,
     hid_s,
     hid_r,
+    rem_s,
+    rem_r,
     pair_s,
     pair_r,
     chip_s,
@@ -154,22 +167,21 @@
     out_r,
 ):
     layers = 2
-    sequences, length, width = tokens_hbm.shape
+    sequences, _, step, width = tokens_hbm.shape
     units = gate_weight.shape[1]
     main = units // LANES * LANES
     rem = units - main
     total_cols = 2 * main + LANES
-    step = length // chunks
     rows = sequences * step
     items = layers * chunks
     half = width // 2
     chips = cb // 2
     size = main // GROUPS
     lines_in = [(0, 2 * size + LANES)]
-    lines_hid = [(0, size + (LANES if rem else 0))]
+    lines_hid = [(0, size)]
     for g in range(1, GROUPS):
         lines_in.append((sum(lines_in[-1]), 2 * size))
-        lines_hid.append((sum(lines_hid[-1]), size))
+        lines_hid.append((g * size + (LANES if rem else 0), size))
     me = lax.axis_index("ra")
     mine = lax.axis_index("cb")
     core = lax.rem(mine, 2)
@@ -199,11 +211,11 @@
             device_id_type=MESH,
         )
 
-    def token_copy(c, s):
+    def token_copy(s):
         return pltpu.make_async_copy(
-            tokens_hbm.at[s, pl.ds(pl.multiple_of(c * step, step), step)],
-            state.at[c, pl.ds(s * step, step)],
-            token_sem.at[c, s],
+            tokens_hbm.at[s],
+            state.at[pl.ds(0, chunks), pl.ds(s * step, step)],
+            token_sem.at[s],
         )
 
     smalls = [
@@ -235,16 +247,13 @@
         )
 
     for s in range(sequences):
-        token_copy(0, s).start()
+        token_copy(s).start()
     smalls[0].start()
     for part in early:
         for kind in range(2):
             load(0, kind, part).start()
     for copy in smalls[1:]:
         copy.start()
-    for c in range(1, chunks):
-        for s in range(sequences):
-            token_copy(c, s).start()
 
     block = 32
 
@@ -308,6 +317,20 @@
         keep = jnp.logical_and(lane >= 2 * rem, lane < 2 * rem + 2)
         return jnp.sum(jnp.where(keep, tile, 0.0), axis=1, keepdims=True)
 
+    def slot_of(k, kind):
+        return k % WINDOW[kind] if isinstance(k, int) else lax.rem(k, WINDOW[kind])
+
+    def launch(k, kind, copies):
+        if not isinstance(k, int):
+
+            @pl.when(k >= WINDOW[kind])
+            def _():
+                for copy in copies:
+                    copy.wait_send()
+
+        for copy in copies:
+            copy.start()
+
     def near_copy(k, first, g):
         to = jnp.where(me == 0, 1, 2)
         passed = jnp.where(me < 2, 1, 0)
@@ -315,8 +338,8 @@
         return pltpu.make_async_remote_copy(
             src_ref=own_part.at[k, r, pl.ds(*lines_in[g])],
             dst_ref=near_part.at[k, r, pl.ds(*lines_in[g])],
-            send_sem=near_s.at[k, 2 * g + int(first)],
-            recv_sem=near_r.at[k, 2 * g + int(first)],
+            send_sem=near_s.at[slot_of(k, "near"), 2 * g + int(first)],
+            recv_sem=near_r.at[slot_of(k, "near"), 2 * g + int(first)],
             device_id={"ra": to},
             device_id_type=MESH,
         )
@@ -325,8 +348,8 @@
         return pltpu.make_async_remote_copy(
             src_ref=far_send.at[k, :, pl.ds(*lines_in[g])],
             dst_ref=far_part.at[k, :, pl.ds(*lines_in[g])],
-            send_sem=far_s.at[k, g],
-            recv_sem=far_r.at[k, g],
+            send_sem=far_s.at[slot_of(k, "far"), g],
+            recv_sem=far_r.at[slot_of(k, "far"), g],
             device_id={"ra": 3 - me},
             device_id_type=MESH,
         )
@@ -338,8 +361,18 @@
         return pltpu.make_async_remote_copy(
             src_ref=hidden.at[k, hid_rows(seq), pl.ds(*lines_hid[g])],
             dst_ref=hidden.at[k, hid_rows(seq), pl.ds(*lines_hid[g])],
-            send_sem=hid_s.at[k, (d - 1) * GROUPS + g],
-            recv_sem=hid_r.at[k, seq * GROUPS + g],
+            send_sem=hid_s.at[slot_of(k, "hid"), (d - 1) * GROUPS + g],
+            recv_sem=hid_r.at[slot_of(k, "hid"), seq * GROUPS + g],
+            device_id={"ra": lax.rem(me + d, ra)},
+            device_id_type=MESH,
+        )
+
+    def rem_copy(k, d, seq):
+        return pltpu.make_async_remote_copy(
+            src_ref=hid_rem.at[k, seq],
+            dst_ref=hid_rem.at[k, seq],
+            send_sem=rem_s.at[slot_of(k, "hid"), d - 1],
+            recv_sem=rem_r.at[slot_of(k, "hid"), seq],
             device_id={"ra": lax.rem(me + d, ra)},
             device_id_type=MESH,
         )
@@ -348,8 +381,8 @@
         return pltpu.make_async_remote_copy(
             src_ref=pair_send.at[k],
             dst_ref=pair_recv.at[k],
-            send_sem=pair_s.at[k],
-            recv_sem=pair_r.at[k],
+            send_sem=pair_s.at[slot_of(k, "pair")],
+            recv_sem=pair_r.at[slot_of(k, "pair")],
             device_id={"cb": 2 * chip + 1 - core},
             device_id_type=MESH,
         )
@@ -358,8 +391,8 @@
         return pltpu.make_async_remote_copy(
             src_ref=chip_part.at[k, chip],
             dst_ref=chip_part.at[k, chip],
-            send_sem=chip_s.at[k, d - 1],
-            recv_sem=chip_r.at[k, d - 1],
+            send_sem=chip_s.at[slot_of(k, "chip"), d - 1],
+            recv_sem=chip_r.at[slot_of(k, "chip"), d - 1],
             device_id={"cb": 2 * lax.rem(chip + d, chips) + core},
             device_id_type=MESH,
         )
@@ -368,8 +401,8 @@
         return pltpu.make_async_remote_copy(
             src_ref=chip_part.at[k, chip],
             dst_ref=chip_part.at[k, lax.rem(chip - d + chips, chips)],
-            send_sem=chip_s.at[k, d - 1],
-            recv_sem=chip_r.at[k, d - 1],
+            send_sem=chip_s.at[slot_of(k, "chip"), d - 1],
+            recv_sem=chip_r.at[slot_of(k, "chip"), d - 1],
             device_id={"cb": 2 * lax.rem(chip + d, chips) + core},
             device_id_type=MESH,
         )
@@ -378,19 +411,14 @@
         return pltpu.make_async_remote_copy(
             src_ref=state.at[k + chunks, :, cols],
             dst_ref=state.at[k + chunks, :, cols],
-            send_sem=out_s.at[k],
-            recv_sem=out_r.at[k],
+            send_sem=out_s.at[slot_of(k, "out")],
+            recv_sem=out_r.at[slot_of(k, "out")],
             device_id={"cb": 2 * chip + 1 - core},
             device_id_type=MESH,
         )
 
     def scaled_rows(k):
         layer = k // chunks
-
-        @pl.when(k < chunks)
-        def _():
-            for s in range(sequences):
-                token_copy(k, s).wait()
 
         values = state[k].astype(jnp.float32)
         squares = jnp.sum(values * values, axis=1, keepdims=True)
@@ -421,8 +449,7 @@
     def send_near(k, g, which=(True, False)):
         @pl.when(outer)
         def _():
-            for first in which:
-                near_copy(k, first, g).start()
+            launch(k, "near", [near_copy(k, first, g) for first in which])
 
     def enter(k):
         @pl.when(k > 0)
@@ -452,7 +479,7 @@
                 far_send[k, :, plain : plain + LANES] = put_squares(
                     tile, get_squares(tile)
                 ).astype(jnp.bfloat16)
-            far_copy(k, g).start()
+            launch(k, "far", [far_copy(k, g)])
 
     def act(k):
         layer = k // chunks
@@ -481,7 +508,7 @@
                 conv = conv + param(3 + j) * conv_pad[first : first + step, start:stop]
             conv_pad[0:8, start:stop] = conv_pad[step : step + 8, start:stop]
             value = conv / (1.0 + jnp.exp(-conv)) * (up * inverse_rms * param(1))
-            hidden[k, r, start:stop] = value.astype(jnp.bfloat16)
+            return value
 
         cols = 256
         inverse_rms = None
@@ -494,14 +521,21 @@
                 inverse_rms = lax.rsqrt(get_squares(tile) / (width * ra) + eps)
                 if rem:
                     up = pltpu.roll(tile, LANES - rem, axis=1)
-                    piece(inverse_rms, tile, up, size, size + LANES)
+                    value = piece(inverse_rms, tile, up, size, size + LANES)
+                    packed = value[: step // 2] + pltpu.roll(value[step // 2 :], rem, axis=1)
+                    hid_rem[k, own_seq] = packed.astype(jnp.bfloat16)
             for start in range(0, size, cols):
                 stop = min(start + cols, size)
                 gate = total(begin + start, begin + stop)
                 up = total(begin + size + start, begin + size + stop)
-                piece(inverse_rms, gate, up, to + start, to + stop)
+                value = piece(inverse_rms, gate, up, to + start, to + stop)
+                hidden[k, r, to + start : to + stop] = value.astype(jnp.bfloat16)
+            copies = []
             for d in (2, 1, 3):
-                hid_copy(k, d, own_seq, g).start()
+                if rem and g == 0:
+                    copies.append(rem_copy(k, d, own_seq))
+                copies.append(hid_copy(k, d, own_seq, g))
+            launch(k, "hid", copies)
 
     def down(k):
         layer = k // chunks
@@ -509,19 +543,29 @@
 
             @pl.when(jnp.logical_not(jnp.logical_and(inner, own_seq == seq)))
             def _():
+                if rem:
+                    rem_copy(k, 1, seq).wait_recv()
                 for g in range(GROUPS):
                     hid_copy(k, 1, seq, g).wait_recv()
 
+        if rem:
+            for seq in range(sequences):
+                packed = hid_rem[k, seq].astype(jnp.float32)
+                for part in range(2):
+                    first = seq * step + part * (step // 2)
+                    rows_of[first : first + step // 2, :] = (
+                        pltpu.roll(packed, LANES - rem, axis=1) if part else packed
+                    )
+            hidden[k, :, size : size + LANES] = rows_of[...].astype(jnp.bfloat16)
         value = jnp.dot(hidden[k], out_w[layer], preferred_element_type=jnp.float32)
         pair_send[k] = value[:, :half].astype(jnp.bfloat16)
         down_keep[k] = value[:, half:]
-        pair_copy(k).start()
+        launch(k, "pair", [pair_copy(k)])
 
     def pair(k):
         pair_copy(k).wait_recv()
         chip_part[k, chip] = (down_keep[k] + pair_recv[k].astype(jnp.float32)).astype(jnp.bfloat16)
-        for d in range(1, chips):
-            chip_copy(k, d).start()
+        launch(k, "chip", [chip_copy(k, d) for d in range(1, chips)])
 
     def fold(k):
         layer = k // chunks
@@ -533,7 +577,7 @@
         kept = residual_keep * state[k, :, my_cols].astype(jnp.float32)
         scale = down_scale[pl.ds(layer, 1), my_cols]
         state[k + chunks, :, my_cols] = (kept + total * scale).astype(jnp.bfloat16)
-        out_copy(k, my_cols).start()
+        launch(k, "out", [out_copy(k, my_cols)])
 
     def done(k):
         out_copy(k, other_cols).wait_recv()
@@ -545,6 +589,8 @@
                 out[s, c, :] = state[k + chunks, s * step : (s + 1) * step, :]
 
     smalls[0].wait()
+    for s in range(sequences):
+        token_copy(s).wait()
     first_scaled, first_squares = scaled_rows(0)
     for g in range(GROUPS):
         convert_group(0, g)
@@ -606,25 +652,33 @@
                     def _():
                         (convert_in if kind == "in" else convert_out)(layer)
 
-    @pl.loop(0, items)
-    def _(k):
-        @pl.when(outer)
-        def _():
-            for g in range(GROUPS):
-                near_copy(k, True, g).wait_send()
-                near_copy(k, False, g).wait_send()
-
-        @pl.when(inner)
-        def _():
-            for g in range(GROUPS):
-                far_copy(k, g).wait_send()
-                for d in range(1, ra):
-                    hid_copy(k, d, own_seq, g).wait_send()
-
-        pair_copy(k).wait_send()
-        for d in range(1, chips):
-            chip_copy(k, d).wait_send()
-        out_copy(k, my_cols).wait_send()
+    def drain(kind, make):
+        @pl.loop(max(items - WINDOW[kind], 0), items)
+        def _(k):
+            for copy in make(k):
+                copy.wait_send()
+
+    @pl.when(outer)
+    def _():
+        drain(
+            "near",
+            lambda k: [near_copy(k, f, g) for f in (True, False) for g in range(GROUPS)],
+        )
+
+    @pl.when(inner)
+    def _():
+        drain("far", lambda k: [far_copy(k, g) for g in range(GROUPS)])
+        drain(
+            "hid",
+            lambda k: [
+                hid_copy(k, d, own_seq, g) for d in range(1, ra) for g in range(GROUPS)
+            ]
+            + ([rem_copy(k, d, own_seq) for d in range(1, ra)] if rem else []),
+        )
+
+    drain("pair", lambda k: [pair_copy(k)])
+    drain("chip", lambda k: [chip_copy(k, d) for d in range(1, chips)])
+    drain("out", lambda k: [out_copy(k, my_cols)])
 
 
 def fused_shards(ra, cb, chunks, *operands):
@@ -667,33 +721,38 @@
             pltpu.VMEM((items, step, total_cols), bf16),
             pltpu.VMEM((items, step, total_cols), bf16),
             pltpu.VMEM((items, rows, padded), bf16),
+            pltpu.VMEM((items, sequences, step // 2, LANES), bf16),
             pltpu.VMEM((items, rows, half), f32),
             pltpu.VMEM((items, rows, half), bf16),
             pltpu.VMEM((items, rows, half), bf16),
             pltpu.VMEM((items, chips, rows, half), bf16),
+            pltpu.VMEM((rows, LANES), f32),
             pltpu.VMEM((8 + step, padded), f32),
             pltpu.VMEM((layers, 3 + taps, padded), f32),
             dma((layers, 2 * GROUPS + 3)),
             dma((6,)),
-            dma((chunks, sequences)),
-            dma((items, 2 * GROUPS)),
-            dma((items, 2 * GROUPS)),
-            dma((items, GROUPS)),
-            dma((items, GROUPS)),
-            dma((items, (ra - 1) * GROUPS)),
-            dma((items, sequences * GROUPS)),
-            dma((items,)),
-            dma((items,)),
-            dma((items, chips - 1)),
-            dma((items, chips - 1)),
-            dma((items,)),
-            dma((items,)),
+            dma((sequences,)),
+            dma((WINDOW["near"], 2 * GROUPS)),
+            dma((WINDOW["near"], 2 * GROUPS)),
+            dma((WINDOW["far"], GROUPS)),
+            dma((WINDOW["far"], GROUPS)),
+            dma((WINDOW["hid"], (ra - 1) * GROUPS)),
+            dma((WINDOW["hid"], sequences * GROUPS)),
+            dma((WINDOW["hid"], ra - 1)),
+            dma((WINDOW["hid"], sequences)),
+            dma((WINDOW["pair"],)),
+            dma((WINDOW["pair"],)),
+            dma((WINDOW["chip"], chips - 1)),
+            dma((WINDOW["chip"], chips - 1)),
+            dma((WINDOW["out"],)),
+            dma((WINDOW["out"],)),
         ],
         compiler_params=pltpu.CompilerParams(
             collective_id=0, has_side_effects=True, vmem_limit_bytes=60 * 1024 * 1024
         ),
     )(
-        *operands[:2],
+        tokens.reshape(sequences, chunks, step, width),
+        operands[1],
         jnp.swapaxes(gate_weight, 1, 2),
         operands[3],
         jnp.swapaxes(operands[4], 1, 2),

time: 74.4 us -> 71.3 us (0.958)
  Pallas kernels: 73.2 us -> 70.3 us
    pallas_call x1, Pallas kernels: 73.2 us -> 70.3 us  [fused_shards(): pl.pallas_call(functools.partial(fused, chunks, ra, cb), out_shape=pltpu....]
where the time goes in v4:
time: 71.3 us; the launch traced here: 71.1 us
  Pallas kernels  70.3 us (99%)
  local copies, waits for them, and re-layouts  0.75 us (1%)
    pallas_call x1, Pallas kernels, fused_shards(): pl.pallas_call(functools.partial(fused, chunks, ra, cb), out_shape=pltpu....  70.3 us

profile of v4, /device:TPU:0, one launch (start us, length us, event | category | flops | bytes accessed | tf_op | source)
XLA Modules:
  0.0 71.1 jit_solution(12683811477325006599)
XLA Ops:
  0.0 70.3 %shard_map.100 = bf16[2,128,768]{2,1,0:T(8,128)(2,1)S(1)} custom-call(bf16[2,8,16,768]{3,2,1,0:T(8,128)(2,1)} %bitcast.6, f32[2,768]{1,0:T(2,128)} %norm_gain_hbm.1, f32[2,1056,768]{2,1,0:T(8,128)} %bitcast.4, f32[2,1056]{1,0:T(2,128)} %gate_scale_hbm.1, f32[2,1056,768]{2,1,0:T(8,128)} %bitcast.5, f32[2,1056]{1,0:T(2,128)} %up_scale_hbm.1, ...), custom_call_target="tpu_custom_call" | custom-call | tf_op jit(solution)/shard_map/pallas_call | solution.py:701
  70.3 0.7 %copy.12 = bf16[2,128,768]{2,1,0:T(8,128)(2,1)} copy(bf16[2,128,768]{2,1,0:T(8,128)(2,1)S(1)} %shard_map.100) | data formatting | bytes 786432

commit v5 on v4

--- a/solution.py
+++ b/solution.py
@@ -104,7 +104,7 @@
     ("pair", 5),
     ("down", 4),
 )
-WINDOW = dict(near=6, far=5, hid=6, pair=5, chip=8, out=4)
+WINDOW = dict(near=5, far=4, hid=5, pair=4, chip=6, out=2)
 CONVERT = {1: ("out", 0), 3: ("in", 1), 5: ("out", 1)}
 
 
@@ -320,16 +320,35 @@
     def slot_of(k, kind):
         return k % WINDOW[kind] if isinstance(k, int) else lax.rem(k, WINDOW[kind])
 
-    def launch(k, kind, copies):
-        if not isinstance(k, int):
+    def launch(k, kind, copies, opens=True):
+        if opens and not isinstance(k, int):
 
             @pl.when(k >= WINDOW[kind])
             def _():
-                for copy in copies:
-                    copy.wait_send()
+                sent(k, kind)
 
         for copy in copies:
             copy.start()
+
+    def take(ref, sem):
+        pltpu.make_async_copy(ref, ref, sem).wait()
+
+    def sent(k, kind):
+        if kind == "near":
+            take(own_part.at[k], near_s.at[slot_of(k, kind)])
+        if kind == "far":
+            take(far_send.at[k], far_s.at[slot_of(k, kind)])
+        if kind == "hid":
+            wide = (ra - 1) * main // sequences
+            take(own_part.at[k, :, pl.ds(0, wide)], hid_s.at[slot_of(k, kind)])
+            if rem:
+                take(hid_rem.at[pl.ds(0, ra - 1), 0], rem_s.at[slot_of(k, kind)])
+        if kind == "pair":
+            take(pair_send.at[k], pair_s.at[slot_of(k, kind)])
+        if kind == "chip":
+            take(chip_part.at[k, pl.ds(0, chips - 1)], chip_s.at[slot_of(k, kind)])
+        if kind == "out":
+            take(state.at[k, :, my_cols], out_s.at[slot_of(k, kind)])
 
     def near_copy(k, first, g):
         to = jnp.where(me == 0, 1, 2)
@@ -338,7 +357,7 @@
         return pltpu.make_async_remote_copy(
             src_ref=own_part.at[k, r, pl.ds(*lines_in[g])],
             dst_ref=near_part.at[k, r, pl.ds(*lines_in[g])],
-            send_sem=near_s.at[slot_of(k, "near"), 2 * g + int(first)],
+            send_sem=near_s.at[slot_of(k, "near")],
             recv_sem=near_r.at[slot_of(k, "near"), 2 * g + int(first)],
             device_id={"ra": to},
             device_id_type=MESH,
@@ -348,7 +367,7 @@
         return pltpu.make_async_remote_copy(
             src_ref=far_send.at[k, :, pl.ds(*lines_in[g])],
             dst_ref=far_part.at[k, :, pl.ds(*lines_in[g])],
-            send_sem=far_s.at[slot_of(k, "far"), g],
+            send_sem=far_s.at[slot_of(k, "far")],
             recv_sem=far_r.at[slot_of(k, "far"), g],
             device_id={"ra": 3 - me},
             device_id_type=MESH,
@@ -361,8 +380,8 @@
         return pltpu.make_async_remote_copy(
             src_ref=hidden.at[k, hid_rows(seq), pl.ds(*lines_hid[g])],
             dst_ref=hidden.at[k, hid_rows(seq), pl.ds(*lines_hid[g])],
-            send_sem=hid_s.at[slot_of(k, "hid"), (d - 1) * GROUPS + g],
-            recv_sem=hid_r.at[slot_of(k, "hid"), seq * GROUPS + g],
+            send_sem=hid_s.at[slot_of(k, "hid")],
+            recv_sem=hid_r.at[slot_of(k, "hid"), seq],
             device_id={"ra": lax.rem(me + d, ra)},
             device_id_type=MESH,
         )
@@ -371,7 +390,7 @@
         return pltpu.make_async_remote_copy(
             src_ref=hid_rem.at[k, seq],
             dst_ref=hid_rem.at[k, seq],
-            send_sem=rem_s.at[slot_of(k, "hid"), d - 1],
+            send_sem=rem_s.at[slot_of(k, "hid")],
             recv_sem=rem_r.at[slot_of(k, "hid"), seq],
             device_id={"ra": lax.rem(me + d, ra)},
             device_id_type=MESH,
@@ -391,18 +410,8 @@
         return pltpu.make_async_remote_copy(
             src_ref=chip_part.at[k, chip],
             dst_ref=chip_part.at[k, chip],
-            send_sem=chip_s.at[slot_of(k, "chip"), d - 1],
-            recv_sem=chip_r.at[slot_of(k, "chip"), d - 1],
-            device_id={"cb": 2 * lax.rem(chip + d, chips) + core},
-            device_id_type=MESH,
-        )
-
-    def chip_wait(k, d):
-        return pltpu.make_async_remote_copy(
-            src_ref=chip_part.at[k, chip],
-            dst_ref=chip_part.at[k, lax.rem(chip - d + chips, chips)],
-            send_sem=chip_s.at[slot_of(k, "chip"), d - 1],
-            recv_sem=chip_r.at[slot_of(k, "chip"), d - 1],
+            send_sem=chip_s.at[slot_of(k, "chip")],
+            recv_sem=chip_r.at[slot_of(k, "chip")],
             device_id={"cb": 2 * lax.rem(chip + d, chips) + core},
             device_id_type=MESH,
         )
@@ -449,7 +458,8 @@
     def send_near(k, g, which=(True, False)):
         @pl.when(outer)
         def _():
-            launch(k, "near", [near_copy(k, first, g) for first in which])
+            copies = [near_copy(k, first, g) for first in which]
+            launch(k, "near", copies, g == 0 and which[0])
 
     def enter(k):
         @pl.when(k > 0)
@@ -479,7 +489,7 @@
                 far_send[k, :, plain : plain + LANES] = put_squares(
                     tile, get_squares(tile)
                 ).astype(jnp.bfloat16)
-            launch(k, "far", [far_copy(k, g)])
+            launch(k, "far", [far_copy(k, g)], g == 0)
 
     def act(k):
         layer = k // chunks
@@ -535,7 +545,7 @@
                 if rem and g == 0:
                     copies.append(rem_copy(k, d, own_seq))
                 copies.append(hid_copy(k, d, own_seq, g))
-            launch(k, "hid", copies)
+            launch(k, "hid", copies, g == 0)
 
     def down(k):
         layer = k // chunks
@@ -545,8 +555,8 @@
             def _():
                 if rem:
                     rem_copy(k, 1, seq).wait_recv()
-                for g in range(GROUPS):
-                    hid_copy(k, 1, seq, g).wait_recv()
+                r = hid_rows(seq)
+                take(own_part.at[k, r, pl.ds(0, main)], hid_r.at[slot_of(k, "hid"), seq])
 
         if rem:
             for seq in range(sequences):
@@ -569,8 +579,7 @@
 
     def fold(k):
         layer = k // chunks
-        for d in range(1, chips):
-            chip_wait(k, d).wait_recv()
+        take(chip_part.at[k, pl.ds(0, chips - 1)], chip_r.at[slot_of(k, "chip")])
         total = chip_part[k, 0].astype(jnp.float32)
         for g in range(1, chips):
             total = total + chip_part[k, g].astype(jnp.float32)
@@ -652,33 +661,22 @@
                     def _():
                         (convert_in if kind == "in" else convert_out)(layer)
 
-    def drain(kind, make):
+    def drain(kind):
         @pl.loop(max(items - WINDOW[kind], 0), items)
         def _(k):
-            for copy in make(k):
-                copy.wait_send()
+            sent(k, kind)
 
     @pl.when(outer)
     def _():
-        drain(
-            "near",
-            lambda k: [near_copy(k, f, g) for f in (True, False) for g in range(GROUPS)],
-        )
+        drain("near")
 
     @pl.when(inner)
     def _():
-        drain("far", lambda k: [far_copy(k, g) for g in range(GROUPS)])
-        drain(
-            "hid",
-            lambda k: [
-                hid_copy(k, d, own_seq, g) for d in range(1, ra) for g in range(GROUPS)
-            ]
-            + ([rem_copy(k, d, own_seq) for d in range(1, ra)] if rem else []),
-        )
-
-    drain("pair", lambda k: [pair_copy(k)])
-    drain("chip", lambda k: [chip_copy(k, d) for d in range(1, chips)])
-    drain("out", lambda k: [out_copy(k, my_cols)])
+        drain("far")
+        drain("hid")
+
+    for kind in ("pair", "chip", "out"):
+        drain(kind)
 
 
 def fused_shards(ra, cb, chunks, *operands):
@@ -732,18 +730,18 @@
             dma((layers, 2 * GROUPS + 3)),
             dma((6,)),
             dma((sequences,)),
+            dma((WINDOW["near"],)),
             dma((WINDOW["near"], 2 * GROUPS)),
-            dma((WINDOW["near"], 2 * GROUPS)),
+            dma((WINDOW["far"],)),
             dma((WINDOW["far"], GROUPS)),
-            dma((WINDOW["far"], GROUPS)),
-            dma((WINDOW["hid"], (ra - 1) * GROUPS)),
-            dma((WINDOW["hid"], sequences * GROUPS)),
-            dma((WINDOW["hid"], ra - 1)),
+            dma((WINDOW["hid"],)),
+            dma((WINDOW["hid"], sequences)),
+            dma((WINDOW["hid"],)),
             dma((WINDOW["hid"], sequences)),
             dma((WINDOW["pair"],)),
             dma((WINDOW["pair"],)),
-            dma((WINDOW["chip"], chips - 1)),
-            dma((WINDOW["chip"], chips - 1)),
+            dma((WINDOW["chip"],)),
+            dma((WINDOW["chip"],)),
             dma((WINDOW["out"],)),
             dma((WINDOW["out"],)),
         ],

time: 71.3 us -> 69.9 us (0.980)
  Pallas kernels: 70.3 us -> 69 us
    pallas_call x1, Pallas kernels: 70.3 us -> 69 us  [fused_shards(): pl.pallas_call(functools.partial(fused, chunks, ra, cb), out_shape=pltpu....]
where the time goes in v5:
time: 69.9 us; the launch traced here: 69.7 us
  Pallas kernels  69 us (99%)
  local copies, waits for them, and re-layouts  0.75 us (1%)
    pallas_call x1, Pallas kernels, fused_shards(): pl.pallas_call(functools.partial(fused, chunks, ra, cb), out_shape=pltpu....  69 us

profile of v5, /device:TPU:0, one launch (start us, length us, event | category | flops | bytes accessed | tf_op | source)
XLA Modules:
  0.0 69.7 jit_solution(13070539311640755974)
XLA Ops:
  0.0 69.0 %shard_map.100 = bf16[2,128,768]{2,1,0:T(8,128)(2,1)S(1)} custom-call(bf16[2,8,16,768]{3,2,1,0:T(8,128)(2,1)} %bitcast.6, f32[2,768]{1,0:T(2,128)} %norm_gain_hbm.1, f32[2,1056,768]{2,1,0:T(8,128)} %bitcast.4, f32[2,1056]{1,0:T(2,128)} %gate_scale_hbm.1, f32[2,1056,768]{2,1,0:T(8,128)} %bitcast.5, f32[2,1056]{1,0:T(2,128)} %up_scale_hbm.1, ...), custom_call_target="tpu_custom_call" | custom-call | tf_op jit(solution)/shard_map/pallas_call | solution.py:699
  69.0 0.7 %copy.12 = bf16[2,128,768]{2,1,0:T(8,128)(2,1)} copy(bf16[2,128,768]{2,1,0:T(8,128)(2,1)S(1)} %shard_map.100) | data formatting | bytes 786432

commit v6 on v5

--- a/solution.py
+++ b/solution.py
@@ -105,7 +105,7 @@
     ("down", 4),
 )
 WINDOW = dict(near=5, far=4, hid=5, pair=4, chip=6, out=2)
-CONVERT = {1: ("out", 0), 3: ("in", 1), 5: ("out", 1)}
+CONVERT = {2: ("out", 0), 4: ("in", 1), 7: ("out", 1)}
 
 
 def fused(
@@ -186,6 +186,9 @@
     mine = lax.axis_index("cb")
     core = lax.rem(mine, 2)
     chip = mine // 2
+    others = [lax.rem(chip + d, chips) for d in range(1, chips)]
+    if chips == 4:
+        others = [3 - chip, chip + 1 - 2 * lax.rem(chip, 2), lax.rem(chip + 2, 4)]
     inner = jnp.logical_and(me >= 1, me <= 2)
     outer = jnp.logical_not(inner)
     own_seq = me - 1
@@ -412,7 +415,7 @@
             dst_ref=chip_part.at[k, chip],
             send_sem=chip_s.at[slot_of(k, "chip")],
             recv_sem=chip_r.at[slot_of(k, "chip")],
-            device_id={"cb": 2 * lax.rem(chip + d, chips) + core},
+            device_id={"cb": 2 * others[d - 1] + core},
             device_id_type=MESH,
         )
 

time: 69.9 us -> 69.8 us (level)
  no operation moved by 1% of the time
where the time goes in v6:
time: 69.8 us; the launch traced here: 69.6 us
  Pallas kernels  68.9 us (99%)
  local copies, waits for them, and re-layouts  0.75 us (1%)
    pallas_call x1, Pallas kernels, fused_shards(): pl.pallas_call(functools.partial(fused, chunks, ra, cb), out_shape=pltpu....  68.9 us

profile of v6, /device:TPU:0, one launch (start us, length us, event | category | flops | bytes accessed | tf_op | source)
XLA Modules:
  0.0 69.6 jit_solution(14855679983437058034)
XLA Ops:
  0.0 68.9 %shard_map.100 = bf16[2,128,768]{2,1,0:T(8,128)(2,1)S(1)} custom-call(bf16[2,8,16,768]{3,2,1,0:T(8,128)(2,1)} %bitcast.6, f32[2,768]{1,0:T(2,128)} %norm_gain_hbm.1, f32[2,1056,768]{2,1,0:T(8,128)} %bitcast.4, f32[2,1056]{1,0:T(2,128)} %gate_scale_hbm.1, f32[2,1056,768]{2,1,0:T(8,128)} %bitcast.5, f32[2,1056]{1,0:T(2,128)} %up_scale_hbm.1, ...), custom_call_target="tpu_custom_call" | custom-call | tf_op jit(solution)/shard_map/pallas_call | solution.py:702
  68.9 0.7 %copy.12 = bf16[2,128,768]{2,1,0:T(8,128)(2,1)} copy(bf16[2,128,768]{2,1,0:T(8,128)(2,1)S(1)} %shard_map.100) | data formatting | bytes 786432
